TPU v7x, 32 devices: a whole 2x2x4 slice. The times are simulated.
32 devices in a mesh: grp: 2 (over y), kv: 4 (over z), tp: 4 (over x, core).
Axes of the slice: x: 2, y: 2, z: 4, core: 2. Of those that a mesh axis runs over, the one named last changes fastest.
Arguments:
- tokens: bfloat16 [256, 4, 2048], P(('grp', 'kv'), None, 'tp'), parts along dimension 0, may hold values from -6 to 6
- in_gain: float32 [2048], replicated, may hold values from 0.1 to 1.9
- w_query: bfloat16 [2048, 1024], P('kv', 'tp'), may hold values from -0.125 to 0.125
- w_key: bfloat16 [2048, 1024], P('kv', 'tp'), may hold values from -0.125 to 0.125
- w_value: bfloat16 [2048, 1024], P('kv', 'tp'), may hold values from -0.125 to 0.125
- w_gate: bfloat16 [2048, 1024], P('kv', 'tp'), may hold values from -0.125 to 0.125
- w_beta: bfloat16 [2048, 16], replicated, may hold values from -0.125 to 0.125
- w_decay: bfloat16 [2048, 16], replicated, may hold values from -0.125 to 0.125
- decay_base: float32 [16], P('tp'), may hold values from 0.05 to 1
- out_gain: float32 [64], replicated, may hold values from 0.1 to 1.9
- w_out: bfloat16 [1024, 2048], P('tp', 'kv'), may hold values from -0.1875 to 0.1875
- state: float32 [256, 64, 1024], P(('grp', 'kv'), None, 'tp'), parts along dimension 0, may hold values from -0.8 to 0.8
- prev_keys: bfloat16 [256, 4, 1024], P(('grp', 'kv'), None, 'tp'), parts along dimension 0, may hold values from -6 to 6
- prev_values: bfloat16 [256, 4, 1024], P(('grp', 'kv'), None, 'tp'), parts along dimension 0, may hold values from -6 to 6
- prev_beta: float32 [256, 4, 16], P(('grp', 'kv'), None, 'tp'), parts along dimension 0, may hold values from -6 to 6
- prev_decay: float32 [256, 4, 16], P(('grp', 'kv'), None, 'tp'), parts along dimension 0, may hold values from -1 to -0.02
- accepted: int32 [256], P(('grp', 'kv')), parts along dimension 0, may hold values from 0 to 4
Outputs:
- mixed: bfloat16 [256, 4, 2048], P(('grp', 'kv'), None, 'tp'), parts along dimension 0
- new_state: float32 [256, 64, 1024], P(('grp', 'kv'), None, 'tp'), parts along dimension 0
There are 2 independent parts, one for each index of `grp`. A program takes and returns all parts, laid end to end along the dimension named above; an argument that names none is the same for every part. Nothing has to cross between parts.
All inputs are finite; a program needn't handle non-finite values.
Results may differ from a plain program's by a relative error of at most 0.012.
Values may be sent and summed in bfloat16 or wider, within the bound.
A program may use at most 128 MiB of HBM per device.

v0:
```python
import functools

import jax
import jax.numpy as jnp
from jax import lax
from jax.experimental import pallas as pl
from jax.experimental.pallas import tpu as pltpu
from jax.sharding import PartitionSpec as P

EPS = 1e-06
F32 = jnp.float32
BF16 = jnp.bfloat16
MESH = pl.DeviceIdType.MESH


def kernel(
    cfg,
    tok_hbm, gain_hbm, wq_hbm, wk_hbm, wv_hbm, wg_hbm, wb_hbm, wd_hbm, base_hbm, og_hbm, wo_hbm,
    state_hbm, pk_hbm, pv_hbm, pb_hbm, pd_hbm, acc_hbm,
    mixed_ref, new_hbm,
    gain_ref, wb_ref, wd_ref, base_ref, og_ref, pk_ref, pv_ref, pb_ref, pd_ref, acc_ref, tok, wp, wo, st, normed, kq, res, tk, up, al, rows_a, rows_b, proj, send_buf, recv_buf, gate_buf, own_share,
    in_sem, own_sem, zr_send, zl_send, z_recv, y_send, y_recv, t_send, t_recv, r_send, r_recv,
    out_sem, small_sem,
):
    n_grp, n_kv, n_tp, seqs, props, heads, hd, gather_out = cfg
    width = heads * hd
    g = lax.axis_index("grp")
    k = lax.axis_index("kv")
    t_me = lax.axis_index("tp")
    rows = seqs * props
    own_rows = wk_hbm.shape[0]
    piece = own_rows // n_grp
    out_piece = wo.shape[1] // n_grp
    sources = [wk_hbm, wq_hbm, wv_hbm, wg_hbm]
    n_mat = len(sources) + (1 if gather_out else 0)

    tok_in = pltpu.make_async_copy(tok_hbm, tok.at[t_me], in_sem.at[0])
    tok_in.start()
    own_copies = []
    for m in range(n_mat):
        if m < len(sources):
            dst = wp.at[m, pl.ds(k * own_rows, own_rows), :]
            copy = pltpu.make_async_copy(sources[m], dst, own_sem.at[m])
        else:
            copy = pltpu.make_async_copy(wo_hbm, wo.at[k], own_sem.at[m])
        copy.start()
        own_copies.append(copy)
    early, late = [], []
    pairs = [
        (pk_hbm, pk_ref, early), (pv_hbm, pv_ref, early), (pb_hbm, pb_ref, early),
        (pd_hbm, pd_ref, early), (acc_hbm, acc_ref, early), (gain_hbm, gain_ref, late),
        (wb_hbm, wb_ref, late), (wd_hbm, wd_ref, late), (base_hbm, base_ref, late),
        (og_hbm, og_ref, late),
    ]
    for i, (src, dst, group) in enumerate(pairs):
        copy = pltpu.make_async_copy(src, dst, small_sem.at[i])
        copy.start()
        group.append(copy)
    state_in = pltpu.make_async_copy(state_hbm, st, in_sem.at[1])
    state_in.start()
    out_in = None
    if not gather_out:
        out_in = pltpu.make_async_copy(wo_hbm, wo, own_sem.at[n_mat])
        out_in.start()

    barrier = pltpu.get_barrier_semaphore()

    def greet(dev):
        pl.semaphore_signal(barrier, inc=1, device_id=dev, device_id_type=MESH)

    @pl.when(k > 0)
    def _():
        greet({"kv": k - 1})

    @pl.when(k < n_kv - 1)
    def _():
        greet({"kv": k + 1})

    for d in range(1, n_grp):
        greet({"grp": lax.rem(g + d, n_grp)})
    for d in range(1, n_tp):
        greet({"tp": lax.rem(t_me + d, n_tp)})

    beside = jnp.minimum(k, 1) + jnp.minimum(n_kv - 1 - k, 1)
    pl.semaphore_wait(barrier, n_grp + n_tp - 2 + beside)

    def slot(m, origin, part):
        if m < len(sources):
            return wp.at[m, pl.ds(origin * own_rows + part * piece, piece), :]
        return wo.at[origin, pl.ds(part * out_piece, out_piece), :]

    def z_right(m, origin):
        ref = slot(m, origin, g)
        return pltpu.make_async_remote_copy(
            ref, ref, zr_send.at[m, origin], z_recv.at[m, origin],
            device_id={"kv": k + 1}, device_id_type=MESH)

    def z_left(m, origin):
        ref = slot(m, origin, g)
        return pltpu.make_async_remote_copy(
            ref, ref, zl_send.at[m, origin], z_recv.at[m, origin],
            device_id={"kv": k - 1}, device_id_type=MESH)

    def y_copy(m, origin, d):
        ref = slot(m, origin, g)
        return pltpu.make_async_remote_copy(
            ref, ref, y_send.at[d - 1, m, origin], y_recv.at[d - 1, m, origin],
            device_id={"grp": lax.rem(g + d, n_grp)}, device_id_type=MESH)

    def y_wait(m, origin, d):
        ref = slot(m, origin, lax.rem(g + n_grp - d, n_grp))
        pltpu.make_async_remote_copy(
            ref, ref, y_send.at[d - 1, m, origin], y_recv.at[d - 1, m, origin],
            device_id={"grp": lax.rem(g + d, n_grp)}, device_id_type=MESH).wait_recv()

    def send_own(m):
        own_copies[m].wait()

        @pl.when(k < n_kv - 1)
        def _():
            z_right(m, k).start()

        @pl.when(k > 0)
        def _():
            z_left(m, k).start()

    def forward_step(m, s):
        left = k - 1 - s
        right = k + 1 + s

        @pl.when(left >= 0)
        def _():
            z_right(m, left).wait_recv()

            @pl.when(k < n_kv - 1)
            def _():
                z_right(m, left).start()

            for d in range(1, n_grp):
                y_copy(m, left, d).start()

        @pl.when(right < n_kv)
        def _():
            z_left(m, right).wait_recv()

            @pl.when(k > 0)
            def _():
                z_left(m, right).start()

            for d in range(1, n_grp):
                y_copy(m, right, d).start()

    def forward(m):
        def step(s, carry):
            forward_step(m, s)
            return carry

        lax.fori_loop(0, n_kv - 1, step, 0)

    def wait_y(m):
        def step(o, carry):
            @pl.when(o != k)
            def _():
                for d in range(1, n_grp):
                    y_wait(m, o, d)

            return carry

        lax.fori_loop(0, n_kv, step, 0)

    def t_copy(d):
        return pltpu.make_async_remote_copy(
            tok.at[t_me], tok.at[t_me], t_send.at[d - 1], t_recv.at[d - 1],
            device_id={"tp": lax.rem(t_me + d, n_tp)}, device_id_type=MESH)

    def t_wait(d):
        origin = lax.rem(t_me + n_tp - d, n_tp)
        pltpu.make_async_remote_copy(
            tok.at[origin], tok.at[origin], t_send.at[d - 1], t_recv.at[d - 1],
            device_id={"tp": lax.rem(t_me + d, n_tp)}, device_id_type=MESH).wait_recv()

    send_own(0)
    tok_in.wait()
    for d in range(1, n_tp):
        t_copy(d).start()
    send_own(1)
    send_own(2)

    blk = (
        lax.broadcasted_iota(jnp.int32, (width, width), 0) // hd
        == lax.broadcasted_iota(jnp.int32, (width, width), 1) // hd
    ).astype(F32).astype(BF16)
    lane_head = lax.broadcasted_iota(jnp.int32, (1, width), 1) // hd
    masks = [(lane_head == h).astype(F32) for h in range(heads)]

    def head_sum(x):
        hi = x.astype(BF16)
        lo = (x - hi.astype(F32)).astype(BF16)
        return jnp.dot(hi, blk, preferred_element_type=F32) + jnp.dot(
            lo, blk, preferred_element_type=F32)

    lanes = 128
    blocks = width // lanes

    def rd(ref, at, *lead):
        return jnp.concatenate([ref[(*lead, c, at)] for c in range(blocks)], axis=-1)

    def wr(ref, at, x, *lead):
        for c in range(blocks):
            ref[(*lead, c, at)] = x[:, c * lanes : (c + 1) * lanes]

    every = pl.ds(0, rows)

    pad = 2 * props

    def by_state(s, carry):
        tile = st[pl.ds(pl.multiple_of(s * hd, hd), hd), :]
        stacked = jnp.concatenate([(tile * mask).astype(BF16) for mask in masks], axis=0)
        at = pl.ds(pl.multiple_of(s * pad, pad), pad)
        lhs = rd(kq, at).astype(BF16)
        wr(res, at, jnp.dot(lhs, stacked, preferred_element_type=F32))
        return carry

    def solve(keys, values, weights, logs, queries):
        cumul = []
        run = None
        for t in range(props):
            run = logs[t] if run is None else run + logs[t]
            cumul.append(run)
        low = [(i, j) for i in range(props) for j in range(i)]
        products = [keys[i] * keys[j] for i, j in low]
        full = []
        if queries is not None:
            full = [(i, j) for i in range(props) for j in range(i + 1)]
            products += [queries[i] * keys[j] for i, j in full]
        sums = head_sum(jnp.concatenate(products, axis=0))
        sums = [sums[i * seqs : (i + 1) * seqs] for i in range(len(products))]
        kk = dict(zip(low, sums))
        qk = dict(zip(full, sums[len(low):]))
        dec = {pair: jnp.exp(cumul[pair[0]] - cumul[pair[1]]) for pair in low}
        growth = [jnp.exp(c) for c in cumul]
        update = []
        for t in range(props):
            seen = rd(res, pl.ds(t, seqs, stride=pad))
            term = values[t] - growth[t] * seen
            for j in range(t):
                term = term - kk[t, j] * dec[t, j] * update[j]
            update.append(weights[t] * term)
        outs = []
        if queries is not None:
            for t in range(props):
                out = growth[t] * rd(res, pl.ds(props + t, seqs, stride=pad))
                for j in range(t + 1):
                    score = qk[t, j] if j == t else qk[t, j] * dec[t, j]
                    out = out + score * update[j]
                outs.append(out)
        return cumul, growth, update, outs

    def split(ref):
        return [rd(ref, pl.ds(t, seqs, stride=props)) for t in range(props)]

    for copy in early:
        copy.wait()
    pk = pk_ref[...].astype(F32).reshape(rows, width)
    wr(rows_a, every, pk * lax.rsqrt(head_sum(pk * pk) + EPS))
    wr(rows_b, every, pv_ref[...].astype(F32).reshape(rows, width))
    keys = split(rows_a)
    values = split(rows_b)
    own_head = (
        lax.broadcasted_iota(jnp.int32, (heads, width), 0)
        == lax.broadcasted_iota(jnp.int32, (heads, width), 1) // hd
    ).astype(F32)

    def over_lanes(x):
        return lax.dot_general(
            x, own_head, (((0,), (0,)), ((), ())),
            precision=lax.Precision.HIGHEST, preferred_element_type=F32)

    weights, logs = [], []
    for t in range(props):
        live = (acc_ref[...] > t).astype(F32)
        weights.append(over_lanes(jax.nn.sigmoid(pb_ref[t]) * live))
        logs.append(over_lanes(pd_ref[t] * live))
        wr(kq, pl.ds(t, seqs, stride=pad), keys[t])
        wr(kq, pl.ds(props + t, seqs, stride=pad), keys[t])
    state_in.wait()
    lax.fori_loop(0, seqs, by_state, 0, unroll=4)
    cumul, growth, update, _ = solve(keys, values, weights, logs, None)
    al[...] = growth[-1]
    for t in range(props):
        wr(tk, pl.ds(t, seqs, stride=pad), jnp.exp(cumul[-1] - cumul[t]) * keys[t])
        wr(up, pl.ds(t, seqs, stride=pad), update[t])
        wr(tk, pl.ds(props + t, seqs, stride=pad), jnp.zeros((seqs, width), F32))
        wr(up, pl.ds(props + t, seqs, stride=pad), jnp.zeros((seqs, width), F32))

    def renew(s, carry):
        at = pl.ds(pl.multiple_of(s * pad, pad), pad)
        outer = lax.dot_general(
            rd(tk, at), rd(up, at), (((0,), (0,)), ((), ())), preferred_element_type=F32)
        where = pl.ds(pl.multiple_of(s * hd, hd), hd)
        tile = al[pl.ds(s, 1), :] * st[where, :]
        for h in range(heads):
            tile = tile + masks[h] * outer[h * hd : (h + 1) * hd, :]
        st[where, :] = tile
        return carry

    forward(0)
    send_own(3)
    lax.fori_loop(0, seqs // 2, renew, 0, unroll=2)
    forward(1)
    if gather_out:
        send_own(n_mat - 1)
    lax.fori_loop(seqs // 2, seqs, renew, 0, unroll=2)
    state_out = pltpu.make_async_copy(st, new_hbm, out_sem)
    state_out.start()

    for d in range(1, n_tp):
        t_wait(d)
    for copy in late:
        copy.wait()
    square = jnp.zeros((rows, 1), F32)
    for i in range(n_tp):
        wide = tok[i].astype(F32).reshape(rows, -1)
        square = square + jnp.sum(wide * wide, -1, keepdims=True)
    feats = tok.shape[3]
    scale = lax.rsqrt(square / (n_tp * feats) + EPS)
    for i in range(n_tp):
        cols = slice(i * feats, (i + 1) * feats)
        normed[:, cols] = (tok[i].astype(F32).reshape(rows, -1) * scale * gain_ref[:, cols]).astype(BF16)
    all_heads = wb_ref.shape[0]
    pick = (
        lax.broadcasted_iota(jnp.int32, (all_heads, width), 0)
        == t_me * heads + lax.broadcasted_iota(jnp.int32, (all_heads, width), 1) // hd
    ).astype(F32)

    def per_head(ref):
        raw = lax.dot_general(
            normed[...], ref[...], (((1,), (1,)), ((), ())), preferred_element_type=F32)
        return jnp.dot(raw, pick, precision=lax.Precision.HIGHEST, preferred_element_type=F32)

    wr(rows_a, every, jax.nn.sigmoid(per_head(wb_ref)))
    weights = split(rows_a)
    base = jnp.zeros((1, width), F32)
    for h in range(heads):
        base = jnp.where(lane_head == h, base_ref[:, h : h + 1], base)
    wr(rows_b, every, -base * jax.nn.softplus(per_head(wd_ref)))
    logs = split(rows_b)

    def project(m):
        return jnp.dot(normed[...], wp[m], preferred_element_type=F32)

    def finish(m):
        wait_y(m)
        if m < len(sources):
            value = project(m)
            if m == 0:
                value = value * lax.rsqrt(head_sum(value * value) + EPS)
            elif m == 1:
                value = value * lax.rsqrt(head_sum(value * value) + EPS) * hd ** (-0.5)
            wr(proj, every, value, m)

    outs = None
    def r_copy(dest):
        return pltpu.make_async_remote_copy(
            send_buf.at[dest], recv_buf.at[t_me], r_send.at[dest], r_recv.at[t_me],
            device_id={"tp": dest}, device_id_type=MESH)

    def r_wait(origin):
        pltpu.make_async_remote_copy(
            send_buf.at[origin], recv_buf.at[origin], r_send.at[origin], r_recv.at[origin],
            device_id={"tp": origin}, device_id_type=MESH).wait_recv()

    def send_share(dest):
        share = jnp.dot(gate_buf[...], wo[dest], preferred_element_type=F32)

        @pl.when(dest == t_me)
        def _():
            own_share[...] = share

        @pl.when(dest != t_me)
        def _():
            send_buf[dest] = share.astype(BF16)
            r_copy(dest).start()

    for m in range(len(sources)):
        if m >= 2:
            forward(m)
        if m >= 1:
            finish(m - 1)
        if m == 3:
            keys = [rd(proj, pl.ds(t, seqs, stride=props), 0) for t in range(props)]
            queries = [rd(proj, pl.ds(t, seqs, stride=props), 1) for t in range(props)]
            values = [rd(proj, pl.ds(t, seqs, stride=props), 2) for t in range(props)]
            for t in range(props):
                wr(kq, pl.ds(t, seqs, stride=pad), keys[t])
                wr(kq, pl.ds(props + t, seqs, stride=pad), queries[t])
            lax.fori_loop(0, seqs, by_state, 0, unroll=4)
            outs = solve(keys, values, weights, logs, queries)[3]
            for t in range(props):
                wr(rows_a, pl.ds(t, seqs, stride=props), outs[t])
            out = rd(rows_a, every)
            out = out * lax.rsqrt(head_sum(out * out) / hd + EPS)
            tile_gain = (
                lax.broadcasted_iota(jnp.int32, (hd, width), 0)
                == lax.broadcasted_iota(jnp.int32, (hd, width), 1) % hd
            ).astype(F32)
            gain = jnp.dot(
                jnp.broadcast_to(og_ref[...], (8, hd)), tile_gain,
                precision=lax.Precision.HIGHEST, preferred_element_type=F32)[:1]
            wr(rows_a, every, out * gain)
    finish(len(sources) - 1)
    gate = rd(proj, every, 3)
    gate_buf[...] = (rd(rows_a, every) * (gate / (1.0 + jnp.exp(-gate)))).astype(BF16)
    if gather_out:
        m = n_mat - 1

        def take(s, carry):
            @pl.when(s < n_kv - 1)
            def _():
                forward_step(m, s)

            @pl.when(k - s >= 0)
            def _():
                @pl.when(s > 0)
                def _():
                    for d in range(1, n_grp):
                        y_wait(m, k - s, d)

                send_share(k - s)

            @pl.when(jnp.logical_and(s > 0, k + s < n_kv))
            def _():
                for d in range(1, n_grp):
                    y_wait(m, k + s, d)
                send_share(k + s)

            return carry

        lax.fori_loop(0, n_kv, take, 0)
    else:
        out_in.wait()
        for d in range(n_tp):
            send_share(lax.rem(t_me + d, n_tp))
    total = own_share[...]
    for d in range(1, n_tp):
        origin = lax.rem(t_me + d, n_tp)
        r_wait(origin)
        total = total + recv_buf[origin].astype(F32)
    mixed_ref[...] = total.reshape(seqs, props, feats).astype(BF16)

    for d in range(1, n_tp):
        t_copy(d).wait_send()
        r_copy(lax.rem(t_me + d, n_tp)).wait_send()

    def drain(m):
        def step(o, carry):
            @pl.when(jnp.logical_and(o <= k, k < n_kv - 1))
            def _():
                z_right(m, o).wait_send()

            @pl.when(jnp.logical_and(o >= k, k > 0))
            def _():
                z_left(m, o).wait_send()

            @pl.when(o != k)
            def _():
                for d in range(1, n_grp):
                    y_copy(m, o, d).wait_send()

            return carry

        lax.fori_loop(0, n_kv, step, 0)

    for m in range(n_mat):
        drain(m)
    state_out.wait()


def body(
    sizes,
    tokens, in_gain, w_query, w_key, w_value, w_gate, w_beta, w_decay, decay_base, out_gain, w_out,
    state, prev_keys, prev_values, prev_beta, prev_decay, accepted,
):
    n_grp, n_kv, n_tp = sizes
    seqs, props, feats = tokens.shape
    heads = decay_base.shape[0]
    hd = out_gain.shape[0]
    width = heads * hd
    rows = seqs * props
    pad = 2 * props
    gather_out = n_kv == n_tp
    if not gather_out:
        w_out = lax.all_gather(w_out, "kv", axis=1, tiled=True)
        w_out = jnp.transpose(w_out.reshape(width, n_tp, feats), (1, 0, 2))
    n_mat = 5 if gather_out else 4
    cfg = (n_grp, n_kv, n_tp, seqs, props, heads, hd, gather_out)
    vmem = pl.BlockSpec(memory_space=pltpu.VMEM)
    hbm = pl.BlockSpec(memory_space=pltpu.HBM)
    args = (
        tokens, in_gain.reshape(1, -1), w_query, w_key, w_value, w_gate,
        w_beta.T, w_decay.T, decay_base.reshape(1, -1), out_gain.reshape(1, -1), w_out,
        state.reshape(seqs * hd, width), prev_keys, prev_values,
        jnp.transpose(prev_beta, (1, 2, 0)), jnp.transpose(prev_decay, (1, 2, 0)),
        accepted.reshape(1, seqs),
    )
    dma = pltpu.SemaphoreType.DMA
    mixed, new_state = pl.pallas_call(
        functools.partial(kernel, cfg),
        out_shape=(
            jax.ShapeDtypeStruct((seqs, props, feats), BF16),
            jax.ShapeDtypeStruct((seqs * hd, width), F32),
        ),
        in_specs=[hbm] * len(args),
        out_specs=(vmem, pl.BlockSpec(memory_space=pl.ANY)),
        scratch_shapes=[
            *[pltpu.VMEM(args[i].shape, args[i].dtype) for i in (1, 6, 7, 8, 9, 12, 13, 14, 15, 16)],
            pltpu.VMEM((n_tp, seqs, props, feats), BF16),
            pltpu.VMEM((4, n_kv * w_key.shape[0], width), BF16),
            pltpu.VMEM((n_tp, width, feats), BF16),
            pltpu.VMEM((seqs * hd, width), F32),
            pltpu.VMEM((rows, n_tp * feats), BF16),
            pltpu.VMEM((width // 128, seqs * pad, 128), F32),
            pltpu.VMEM((width // 128, seqs * pad, 128), F32),
            pltpu.VMEM((width // 128, seqs * pad, 128), F32),
            pltpu.VMEM((width // 128, seqs * pad, 128), F32),
            pltpu.VMEM((seqs, width), F32),
            pltpu.VMEM((width // 128, rows, 128), F32),
            pltpu.VMEM((width // 128, rows, 128), F32),
            pltpu.VMEM((4, width // 128, rows, 128), F32),
            pltpu.VMEM((n_tp, rows, feats), BF16),
            pltpu.VMEM((n_tp, rows, feats), BF16),
            pltpu.VMEM((rows, width), BF16),
            pltpu.VMEM((rows, feats), F32),
            dma((2,)),
            dma((6,)),
            dma((n_mat, n_kv)),
            dma((n_mat, n_kv)),
            dma((n_mat, n_kv)),
            dma((max(n_grp - 1, 1), n_mat, n_kv)),
            dma((max(n_grp - 1, 1), n_mat, n_kv)),
            dma((n_tp - 1,)),
            dma((n_tp - 1,)),
            dma((n_tp,)),
            dma((n_tp,)),
            dma(()),
            dma((10,)),
        ],
        compiler_params=pltpu.CompilerParams(
            collective_id=0, has_side_effects=True, vmem_limit_bytes=67043328),
    )(*args)
    return mixed, new_state.reshape(seqs, hd, width)


def solution(mesh):
    sizes = (mesh.shape["grp"], mesh.shape["kv"], mesh.shape["tp"])
    tokens = P(("grp", "kv"), None, "tp")
    placed = (
        tokens, P(), P("kv", "tp"), P("kv", "tp"), P("kv", "tp"), P("kv", "tp"), P(), P(),
        P("tp"), P(), P("tp", "kv"), tokens, tokens, tokens, tokens, tokens, P(("grp", "kv")),
    )
    return jax.shard_map(
        functools.partial(body, sizes),
        mesh=mesh,
        in_specs=placed,
        out_specs=(tokens, tokens),
        check_vma=False,
    )
```

profile of v0, /device:TPU:0, one launch (start us, length us, event | category | flops | bytes accessed | tf_op | source)
XLA Modules:
  0.0 72.8 jit_solution(520634901363984867)
XLA Ops:
  0.6 67.4 %shard_map.176 = (bf16[32,4,512]{2,1,0:T(4,128)(2,1)}, f32[2048,256]{1,0:T(8,128)}) custom-call(bf16[32,4,512]{2,1,0:T(4,128)(2,1)} %tok_hbm.1, f32[1,2048]{1,0:T(1,128)} %bitcast.14, bf16[512,256]{1,0:T(8,128)(2,1)} %wq_hbm.1, bf16[512,256]{1,0:T(8,128)(2,1)} %wk_hbm.1, bf16[512,256]{1,0:T(8,128)(2,1)} %wv_hbm.1, bf16[512,256]{1,0:T(8,128)(2,1)} %wg_hbm.1, ...), custom_call_target="tpu_custom_call" | custom-call | tf_op jit(solution)/shard_map/pallas_call | solution.py:507
  68.0 1.6 %copy.21 = bf16[32,4,512]{2,1,0:T(4,128)(2,1)} copy(bf16[32,4,512]{2,1,0:T(4,128)(2,1)} %get-tuple-element.8) | data formatting | bytes 262144
  69.6 3.1 %copy.22 = f32[32,64,256]{2,1,0:T(8,128)} copy(f32[32,64,256]{2,1,0:T(8,128)} %bitcast.11) | data formatting | bytes 4194304
where the time goes:
time: 72.9 us; the launch traced here: 72.8 us
  Pallas kernels  67.4 us (92%)
  local copies, waits for them, and re-layouts  4.73 us (6%)
    pallas_call x1, Pallas kernels, body(): pl.pallas_call(functools.partial(kernel, cfg), out_shape=(jax.ShapeDtypeS...  67.4 us
    unnamed x2, local copies, waits for them, and re-layouts  4.73 us

commit v1 on v0

--- a/solution.py
+++ b/solution.py
@@ -476,6 +476,570 @@
     state_out.wait()
 
 
+def pair_kernel(
+    cfg,
+    tok_hbm, gain_hbm, wq_hbm, wk_hbm, wv_hbm, wg_hbm, wb_hbm, wd_hbm, base_hbm, og_hbm, wo_hbm,
+    state_hbm, pk_hbm, pv_hbm, pb_hbm, pd_hbm, acc_hbm,
+    mixed_ref, new_hbm,
+    gain_ref, wbd_ref, base_ref, og_ref, pk_ref, pv_ref, pb_ref, pd_ref, acc_ref, tok, wp, wo, st, normed, kq, res, tk, up, al, rows_a, rows_b, proj, own_part, part_send, part_recv, small_own, small_send, small_recv, send_buf, recv_buf, gate_buf, own_share,
+    in_sem, own_sem, wz_send, wz_recv, wy_send, wy_recv, t_send, f_send, t_recv, zr_send, zl_send, z_recv, y_send, y_recv, p_send, p_recv, r_send, r_recv,
+    out_sem, small_sem,
+):
+    n_grp, n_kv, n_tp, seqs, props, heads, hd = cfg
+    width = heads * hd
+    g = lax.axis_index("grp")
+    k = lax.axis_index("kv")
+    t_me = lax.axis_index("tp")
+    rows = seqs * props
+    own_rows = wk_hbm.shape[0]
+    piece = own_rows // n_grp
+    out_piece = wo.shape[1] // n_grp
+    feats = tok_hbm.shape[2]
+    sources = [wk_hbm, wq_hbm, wv_hbm, wg_hbm]
+    n_src = len(sources)
+    all_heads = wb_hbm.shape[0]
+    pair = k // 2
+    side = lax.rem(k, 2)
+    mate = k + 1 - 2 * side
+    partner = lax.rem(k + n_kv // 2, n_kv)
+    chip = t_me // 2
+    core = lax.rem(t_me, 2)
+    beside_core = 2 * chip + 1 - core
+    home = lax.rem(pair + chip + 1, 2)
+    g_other = lax.rem(g + 1, n_grp)
+    half_feats = 2 * feats
+
+    own_slot = home * (2 + core) + (1 - home) * 4
+    tok_in = pltpu.make_async_copy(tok_hbm, tok.at[own_slot], in_sem.at[0])
+    tok_in.start()
+    own_copies = []
+    for m in range(n_src + 1):
+        if m < n_src:
+            dst = wp.at[m, pl.ds(side * own_rows, own_rows), :]
+            copy = pltpu.make_async_copy(sources[m], dst, own_sem.at[m])
+        else:
+            copy = pltpu.make_async_copy(wo_hbm, wo.at[k], own_sem.at[m])
+        copy.start()
+        own_copies.append(copy)
+    early, late = [], []
+    ours = pl.ds(pl.multiple_of(pair * half_feats, half_feats), half_feats)
+    pairs = [
+        (pk_hbm, pk_ref, early), (pv_hbm, pv_ref, early), (pb_hbm, pb_ref, early),
+        (pd_hbm, pd_ref, early), (acc_hbm, acc_ref, early),
+        (gain_hbm.at[:, ours], gain_ref, late),
+        (wb_hbm.at[:, ours], wbd_ref.at[pl.ds(0, all_heads), :], late),
+        (wd_hbm.at[:, ours], wbd_ref.at[pl.ds(all_heads, all_heads), :], late),
+        (base_hbm, base_ref, late), (og_hbm, og_ref, late),
+    ]
+    for i, (src, dst, group) in enumerate(pairs):
+        copy = pltpu.make_async_copy(src, dst, small_sem.at[i])
+        copy.start()
+        group.append(copy)
+    state_in = pltpu.make_async_copy(state_hbm, st, in_sem.at[1])
+    state_in.start()
+
+    barrier = pltpu.get_barrier_semaphore()
+
+    def greet(dev):
+        pl.semaphore_signal(barrier, inc=1, device_id=dev, device_id_type=MESH)
+
+    for d in range(1, n_kv):
+        greet({"kv": lax.rem(k + d, n_kv)})
+    for d in range(1, n_tp):
+        greet({"tp": lax.rem(t_me + d, n_tp)})
+    greet({"grp": g_other})
+    far_tp = 2 * (1 - chip) + core
+    greet({"kv": partner, "tp": far_tp})
+    pl.semaphore_wait(barrier, n_kv + n_tp)
+
+    def remote(src, dst, send, recv, dev):
+        return pltpu.make_async_remote_copy(
+            src, dst, send, recv, device_id=dev, device_id_type=MESH)
+
+    to_slot = core + 2 * home
+    to_kv = lax.rem(k + (1 - home) * (n_kv // 2), n_kv)
+    to_tp = 2 * chip + home * (1 - core) + (1 - home) * core
+
+    def tok_far():
+        return remote(tok.at[own_slot], tok.at[to_slot], t_send.at[0], t_recv.at[to_slot],
+                      {"kv": to_kv, "tp": far_tp})
+
+    def tok_near():
+        return remote(tok.at[own_slot], tok.at[to_slot], t_send.at[1], t_recv.at[to_slot],
+                      {"kv": to_kv, "tp": to_tp})
+
+    def tok_relay(j):
+        slot = 2 * j + core
+        return remote(tok.at[slot], tok.at[slot], f_send.at[j], t_recv.at[slot],
+                      {"tp": beside_core})
+
+    def tok_wait(slot):
+        remote(tok.at[slot], tok.at[slot], f_send.at[0], t_recv.at[slot],
+               {"tp": beside_core}).wait_recv()
+
+    def w_slot(m, block, half):
+        return wp.at[m, pl.ds(block * own_rows + half * piece, piece), :]
+
+    def w_mate(m):
+        ref = w_slot(m, side, g)
+        return remote(ref, ref, wz_send.at[m], wz_recv.at[m], {"kv": mate})
+
+    def w_share(m):
+        ref = w_slot(m, 1 - side, g)
+        return remote(ref, ref, wy_send.at[m], wy_recv.at[m], {"grp": g_other})
+
+    def w_pass(m):
+        ref = w_slot(m, 1 - side, g)
+        remote(ref, ref, wz_send.at[m], wz_recv.at[m], {"kv": mate}).wait_recv()
+        w_share(m).start()
+
+    def w_ready(m):
+        ref = w_slot(m, 1 - side, g_other)
+        remote(ref, ref, wy_send.at[m], wy_recv.at[m], {"grp": g_other}).wait_recv()
+
+    def o_slot(origin, part):
+        return wo.at[origin, pl.ds(part * out_piece, out_piece), :]
+
+    def z_right(origin):
+        ref = o_slot(origin, g)
+        return remote(ref, ref, zr_send.at[origin], z_recv.at[origin], {"kv": k + 1})
+
+    def z_left(origin):
+        ref = o_slot(origin, g)
+        return remote(ref, ref, zl_send.at[origin], z_recv.at[origin], {"kv": k - 1})
+
+    def y_copy(origin):
+        ref = o_slot(origin, g)
+        return remote(ref, ref, y_send.at[origin], y_recv.at[origin], {"grp": g_other})
+
+    def y_wait(origin):
+        ref = o_slot(origin, g_other)
+        remote(ref, ref, y_send.at[origin], y_recv.at[origin], {"grp": g_other}).wait_recv()
+
+    def forward_step(s):
+        left = k - 1 - s
+        right = k + 1 + s
+
+        @pl.when(left >= 0)
+        def _():
+            z_right(left).wait_recv()
+
+            @pl.when(k < n_kv - 1)
+            def _():
+                z_right(left).start()
+
+            y_copy(left).start()
+
+        @pl.when(right < n_kv)
+        def _():
+            z_left(right).wait_recv()
+
+            @pl.when(k > 0)
+            def _():
+                z_left(right).start()
+
+            y_copy(right).start()
+
+    def p_copy(m):
+        return remote(part_send.at[m], part_recv.at[m], p_send.at[m], p_recv.at[m],
+                      {"kv": partner})
+
+    def small_copy():
+        return remote(small_send, small_recv, p_send.at[n_src], p_recv.at[n_src],
+                      {"kv": partner})
+
+    tok_in.wait()
+    tok_far().start()
+    tok_near().start()
+    for m in range(n_src):
+        own_copies[m].wait()
+        w_mate(m).start()
+    own_copies[n_src].wait()
+
+    @pl.when(k < n_kv - 1)
+    def _():
+        z_right(k).start()
+
+    @pl.when(k > 0)
+    def _():
+        z_left(k).start()
+
+    blk = (
+        lax.broadcasted_iota(jnp.int32, (width, width), 0) // hd
+        == lax.broadcasted_iota(jnp.int32, (width, width), 1) // hd
+    ).astype(F32).astype(BF16)
+    lane_head = lax.broadcasted_iota(jnp.int32, (1, width), 1) // hd
+    masks = [(lane_head == h).astype(F32) for h in range(heads)]
+
+    def head_sum(x):
+        hi = x.astype(BF16)
+        lo = (x - hi.astype(F32)).astype(BF16)
+        return jnp.dot(hi, blk, preferred_element_type=F32) + jnp.dot(
+            lo, blk, preferred_element_type=F32)
+
+    lanes = 128
+    blocks = width // lanes
+
+    def rd(ref, at, *lead):
+        return jnp.concatenate([ref[(*lead, c, at)] for c in range(blocks)], axis=-1)
+
+    def wr(ref, at, x, *lead):
+        for c in range(blocks):
+            ref[(*lead, c, at)] = x[:, c * lanes : (c + 1) * lanes]
+
+    every = pl.ds(0, rows)
+
+    pad = 2 * props
+
+    def by_state(s, carry):
+        tile = st[pl.ds(pl.multiple_of(s * hd, hd), hd), :]
+        stacked = jnp.concatenate([(tile * mask).astype(BF16) for mask in masks], axis=0)
+        at = pl.ds(pl.multiple_of(s * pad, pad), pad)
+        lhs = rd(kq, at).astype(BF16)
+        wr(res, at, jnp.dot(lhs, stacked, preferred_element_type=F32))
+        return carry
+
+    def solve(keys, values, weights, logs, queries):
+        cumul = []
+        run = None
+        for t in range(props):
+            run = logs[t] if run is None else run + logs[t]
+            cumul.append(run)
+        low = [(i, j) for i in range(props) for j in range(i)]
+        products = [keys[i] * keys[j] for i, j in low]
+        full = []
+        if queries is not None:
+            full = [(i, j) for i in range(props) for j in range(i + 1)]
+            products += [queries[i] * keys[j] for i, j in full]
+        sums = head_sum(jnp.concatenate(products, axis=0))
+        sums = [sums[i * seqs : (i + 1) * seqs] for i in range(len(products))]
+        kk = dict(zip(low, sums))
+        qk = dict(zip(full, sums[len(low):]))
+        dec = {pair: jnp.exp(cumul[pair[0]] - cumul[pair[1]]) for pair in low}
+        growth = [jnp.exp(c) for c in cumul]
+        update = []
+        for t in range(props):
+            seen = rd(res, pl.ds(t, seqs, stride=pad))
+            term = values[t] - growth[t] * seen
+            for j in range(t):
+                term = term - kk[t, j] * dec[t, j] * update[j]
+            update.append(weights[t] * term)
+        outs = []
+        if queries is not None:
+            for t in range(props):
+                out = growth[t] * rd(res, pl.ds(props + t, seqs, stride=pad))
+                for j in range(t + 1):
+                    score = qk[t, j] if j == t else qk[t, j] * dec[t, j]
+                    out = out + score * update[j]
+                outs.append(out)
+        return cumul, growth, update, outs
+
+    def split(ref):
+        return [rd(ref, pl.ds(t, seqs, stride=props)) for t in range(props)]
+
+    for copy in early:
+        copy.wait()
+    pk = pk_ref[...].astype(F32).reshape(rows, width)
+    wr(rows_a, every, pk * lax.rsqrt(head_sum(pk * pk) + EPS))
+    wr(rows_b, every, pv_ref[...].astype(F32).reshape(rows, width))
+    keys = split(rows_a)
+    values = split(rows_b)
+    own_head = (
+        lax.broadcasted_iota(jnp.int32, (heads, width), 0)
+        == lax.broadcasted_iota(jnp.int32, (heads, width), 1) // hd
+    ).astype(F32)
+
+    def over_lanes(x):
+        return lax.dot_general(
+            x, own_head, (((0,), (0,)), ((), ())),
+            precision=lax.Precision.HIGHEST, preferred_element_type=F32)
+
+    weights, logs = [], []
+    for t in range(props):
+        live = (acc_ref[...] > t).astype(F32)
+        weights.append(over_lanes(jax.nn.sigmoid(pb_ref[t]) * live))
+        logs.append(over_lanes(pd_ref[t] * live))
+        wr(kq, pl.ds(t, seqs, stride=pad), keys[t])
+        wr(kq, pl.ds(props + t, seqs, stride=pad), keys[t])
+    state_in.wait()
+    lax.fori_loop(0, seqs, by_state, 0, unroll=4)
+    cumul, growth, update, _ = solve(keys, values, weights, logs, None)
+    al[...] = growth[-1]
+    for t in range(props):
+        wr(tk, pl.ds(t, seqs, stride=pad), jnp.exp(cumul[-1] - cumul[t]) * keys[t])
+        wr(up, pl.ds(t, seqs, stride=pad), update[t])
+        wr(tk, pl.ds(props + t, seqs, stride=pad), jnp.zeros((seqs, width), F32))
+        wr(up, pl.ds(props + t, seqs, stride=pad), jnp.zeros((seqs, width), F32))
+
+    def renew(s, carry):
+        at = pl.ds(pl.multiple_of(s * pad, pad), pad)
+        outer = lax.dot_general(
+            rd(tk, at), rd(up, at), (((0,), (0,)), ((), ())), preferred_element_type=F32)
+        where = pl.ds(pl.multiple_of(s * hd, hd), hd)
+        tile = al[pl.ds(s, 1), :] * st[where, :]
+        for h in range(heads):
+            tile = tile + masks[h] * outer[h * hd : (h + 1) * hd, :]
+        st[where, :] = tile
+        return carry
+
+    w_pass(0)
+
+    @pl.when(home == 0)
+    def _():
+        tok_wait(2 + core)
+        tok_relay(1).start()
+
+    lax.fori_loop(0, seqs // 2, renew, 0, unroll=2)
+    w_pass(1)
+    tok_wait(core)
+    tok_relay(0).start()
+    lax.fori_loop(seqs // 2, seqs, renew, 0, unroll=2)
+    state_out = pltpu.make_async_copy(st, new_hbm, out_sem)
+    state_out.start()
+    for copy in late:
+        copy.wait()
+    w_pass(2)
+    tok_wait(1 - core)
+    tok_wait(3 - core)
+    ones = jnp.ones((8, feats), BF16)
+    squares = jnp.zeros((8, 2 * rows), F32)
+    last = (((1,), (1,)), ((), ()))
+    for c in range(2):
+        cols = slice(c * feats, (c + 1) * feats)
+        wide = jnp.concatenate(
+            [tok[c].astype(F32).reshape(rows, feats), tok[2 + c].astype(F32).reshape(rows, feats)],
+            axis=0)
+        normed[:, cols] = (wide * gain_ref[:, cols]).astype(BF16)
+        sq = wide * wide
+        hi = sq.astype(BF16)
+        lo = (sq - hi.astype(F32)).astype(BF16)
+        squares = squares + lax.dot_general(ones, hi, last, preferred_element_type=F32)
+        squares = squares + lax.dot_general(ones, lo, last, preferred_element_type=F32)
+    raw = lax.dot_general(wbd_ref[...], normed[...], last, preferred_element_type=F32)
+    small = jnp.concatenate([raw, squares], axis=0)
+    small_send[...] = small[:, :rows]
+    small_copy().start()
+    small_own[...] = small[:, rows:]
+
+    def project(m):
+        both = jnp.dot(normed[...], wp[m], preferred_element_type=F32)
+        part_send[m] = both[:rows].astype(BF16)
+        p_copy(m).start()
+        own_part[m] = both[rows:]
+
+    for m in range(n_src):
+        w_ready(m)
+        project(m)
+        if m == 0:
+            w_pass(3)
+        else:
+            forward_step(m - 1)
+
+    pick = (
+        lax.broadcasted_iota(jnp.int32, (all_heads, width), 0)
+        == t_me * heads + lax.broadcasted_iota(jnp.int32, (all_heads, width), 1) // hd
+    ).astype(F32)
+    small_copy().wait_recv()
+    small = small_own[...] + small_recv[...]
+    scale = lax.rsqrt(small[2 * all_heads :] / (n_tp * feats) + EPS)
+    beta = small[:all_heads] * scale[:1]
+    decay = small[all_heads : 2 * all_heads] * scale[:1]
+
+    def spread(x, over):
+        return lax.dot_general(
+            x, over, (((0,), (0,)), ((), ())),
+            precision=lax.Precision.HIGHEST, preferred_element_type=F32)
+
+    wr(rows_a, every, spread(jax.nn.sigmoid(beta), pick))
+    weights = split(rows_a)
+    base = jnp.zeros((1, width), F32)
+    for h in range(heads):
+        base = jnp.where(lane_head == h, base_ref[:, h : h + 1], base)
+    wr(rows_b, every, -base * spread(jax.nn.softplus(decay), pick))
+    logs = split(rows_b)
+    row_scale = spread(
+        scale, (lax.broadcasted_iota(jnp.int32, (8, width), 0) == 0).astype(F32))
+
+    def finish(m):
+        p_copy(m).wait_recv()
+        value = (own_part[m] + part_recv[m].astype(F32)) * row_scale
+        if m == 0:
+            value = value * lax.rsqrt(head_sum(value * value) + EPS)
+        elif m == 1:
+            value = value * lax.rsqrt(head_sum(value * value) + EPS) * hd ** (-0.5)
+        wr(proj, every, value, m)
+
+    def r_copy(dest):
+        return pltpu.make_async_remote_copy(
+            send_buf.at[dest], recv_buf.at[t_me], r_send.at[dest], r_recv.at[t_me],
+            device_id={"tp": dest}, device_id_type=MESH)
+
+    def r_wait(origin):
+        pltpu.make_async_remote_copy(
+            send_buf.at[origin], recv_buf.at[origin], r_send.at[origin], r_recv.at[origin],
+            device_id={"tp": origin}, device_id_type=MESH).wait_recv()
+
+    def send_share(dest):
+        share = jnp.dot(gate_buf[...], wo[dest], preferred_element_type=F32)
+
+        @pl.when(dest == t_me)
+        def _():
+            own_share[...] = share
+
+        @pl.when(dest != t_me)
+        def _():
+            send_buf[dest] = share.astype(BF16)
+            r_copy(dest).start()
+
+    for m in range(3):
+        finish(m)
+    keys = [rd(proj, pl.ds(t, seqs, stride=props), 0) for t in range(props)]
+    queries = [rd(proj, pl.ds(t, seqs, stride=props), 1) for t in range(props)]
+    values = [rd(proj, pl.ds(t, seqs, stride=props), 2) for t in range(props)]
+    for t in range(props):
+        wr(kq, pl.ds(t, seqs, stride=pad), keys[t])
+        wr(kq, pl.ds(props + t, seqs, stride=pad), queries[t])
+    lax.fori_loop(0, seqs, by_state, 0, unroll=4)
+    outs = solve(keys, values, weights, logs, queries)[3]
+    for t in range(props):
+        wr(rows_a, pl.ds(t, seqs, stride=props), outs[t])
+    out = rd(rows_a, every)
+    out = out * lax.rsqrt(head_sum(out * out) / hd + EPS)
+    tile_gain = (
+        lax.broadcasted_iota(jnp.int32, (hd, width), 0)
+        == lax.broadcasted_iota(jnp.int32, (hd, width), 1) % hd
+    ).astype(F32)
+    gain = jnp.dot(
+        jnp.broadcast_to(og_ref[...], (8, hd)), tile_gain,
+        precision=lax.Precision.HIGHEST, preferred_element_type=F32)[:1]
+    wr(rows_a, every, out * gain)
+    finish(n_src - 1)
+    gate = rd(proj, every, 3)
+    gate_buf[...] = (rd(rows_a, every) * (gate / (1.0 + jnp.exp(-gate)))).astype(BF16)
+
+    def take(s, carry):
+        @pl.when(k - s >= 0)
+        def _():
+            @pl.when(s > 0)
+            def _():
+                y_wait(k - s)
+
+            send_share(k - s)
+
+        @pl.when(jnp.logical_and(s > 0, k + s < n_kv))
+        def _():
+            y_wait(k + s)
+            send_share(k + s)
+
+        return carry
+
+    lax.fori_loop(0, n_kv, take, 0)
+    total = own_share[...]
+    for d in range(1, n_tp):
+        origin = lax.rem(t_me + d, n_tp)
+        r_wait(origin)
+        total = total + recv_buf[origin].astype(F32)
+    mixed_ref[...] = total.reshape(seqs, props, feats).astype(BF16)
+
+    tok_far().wait_send()
+    tok_near().wait_send()
+    tok_relay(0).wait_send()
+
+    @pl.when(home == 0)
+    def _():
+        tok_relay(1).wait_send()
+
+    for m in range(n_src):
+        w_mate(m).wait_send()
+        w_share(m).wait_send()
+        p_copy(m).wait_send()
+    small_copy().wait_send()
+    for d in range(1, n_tp):
+        r_copy(lax.rem(t_me + d, n_tp)).wait_send()
+
+    def drain(o, carry):
+        @pl.when(jnp.logical_and(o <= k, k < n_kv - 1))
+        def _():
+            z_right(o).wait_send()
+
+        @pl.when(jnp.logical_and(o >= k, k > 0))
+        def _():
+            z_left(o).wait_send()
+
+        @pl.when(o != k)
+        def _():
+            y_copy(o).wait_send()
+
+        return carry
+
+    lax.fori_loop(0, n_kv, drain, 0)
+    state_out.wait()
+
+
+def pair_call(sizes, args, seqs, props, feats, heads, hd, width, rows, pad):
+    n_grp, n_kv, n_tp = sizes
+    cfg = (n_grp, n_kv, n_tp, seqs, props, heads, hd)
+    vmem = pl.BlockSpec(memory_space=pltpu.VMEM)
+    hbm = pl.BlockSpec(memory_space=pltpu.HBM)
+    dma = pltpu.SemaphoreType.DMA
+    own_rows = args[2].shape[0]
+    all_heads = args[6].shape[0]
+    n_src = 4
+    small = (2 * all_heads + 8, rows)
+    return pl.pallas_call(
+        functools.partial(pair_kernel, cfg),
+        out_shape=(
+            jax.ShapeDtypeStruct((seqs, props, feats), BF16),
+            jax.ShapeDtypeStruct((seqs * hd, width), F32),
+        ),
+        in_specs=[hbm] * len(args),
+        out_specs=(vmem, pl.BlockSpec(memory_space=pl.ANY)),
+        scratch_shapes=[
+            pltpu.VMEM((1, 2 * feats), F32),
+            pltpu.VMEM((2 * all_heads, 2 * feats), BF16),
+            *[pltpu.VMEM(args[i].shape, args[i].dtype) for i in (8, 9, 12, 13, 14, 15, 16)],
+            pltpu.VMEM((5, seqs, props, feats), BF16),
+            pltpu.VMEM((n_src, 2 * own_rows, width), BF16),
+            pltpu.VMEM((n_tp, width, feats), BF16),
+            pltpu.VMEM((seqs * hd, width), F32),
+            pltpu.VMEM((2 * rows, 2 * feats), BF16),
+            pltpu.VMEM((width // 128, seqs * pad, 128), F32),
+            pltpu.VMEM((width // 128, seqs * pad, 128), F32),
+            pltpu.VMEM((width // 128, seqs * pad, 128), F32),
+            pltpu.VMEM((width // 128, seqs * pad, 128), F32),
+            pltpu.VMEM((seqs, width), F32),
+            pltpu.VMEM((width // 128, rows, 128), F32),
+            pltpu.VMEM((width // 128, rows, 128), F32),
+            pltpu.VMEM((n_src, width // 128, rows, 128), F32),
+            pltpu.VMEM((n_src, rows, width), F32),
+            pltpu.VMEM((n_src, rows, width), BF16),
+            pltpu.VMEM((n_src, rows, width), BF16),
+            pltpu.VMEM(small, F32),
+            pltpu.VMEM(small, F32),
+            pltpu.VMEM(small, F32),
+            pltpu.VMEM((n_tp, rows, feats), BF16),
+            pltpu.VMEM((n_tp, rows, feats), BF16),
+            pltpu.VMEM((rows, width), BF16),
+            pltpu.VMEM((rows, feats), F32),
+            dma((2,)),
+            dma((n_src + 1,)),
+            *[dma((n_src,)) for _ in range(4)],
+            dma((2,)),
+            dma((2,)),
+            dma((4,)),
+            *[dma((n_kv,)) for _ in range(5)],
+            dma((n_src + 1,)),
+            dma((n_src + 1,)),
+            dma((n_tp,)),
+            dma((n_tp,)),
+            dma(()),
+            dma((10,)),
+        ],
+        compiler_params=pltpu.CompilerParams(
+            collective_id=1, has_side_effects=True, vmem_limit_bytes=67043328),
+    )(*args)
+
+
 def body(
     sizes,
     tokens, in_gain, w_query, w_key, w_value, w_gate, w_beta, w_decay, decay_base, out_gain, w_out,
@@ -488,6 +1052,9 @@
     width = heads * hd
     rows = seqs * props
     pad = 2 * props
+    paired = (
+        n_grp == 2 and n_kv == n_tp and n_kv // 2 == 2
+        and w_query.shape[0] == feats and w_query.shape[0] * n_kv == in_gain.shape[0])
     gather_out = n_kv == n_tp
     if not gather_out:
         w_out = lax.all_gather(w_out, "kv", axis=1, tiled=True)
@@ -503,6 +1070,10 @@
         jnp.transpose(prev_beta, (1, 2, 0)), jnp.transpose(prev_decay, (1, 2, 0)),
         accepted.reshape(1, seqs),
     )
+    if paired:
+        mixed, new_state = pair_call(
+            sizes, args, seqs, props, feats, heads, hd, width, rows, pad)
+        return mixed, new_state.reshape(seqs, hd, width)
     dma = pltpu.SemaphoreType.DMA
     mixed, new_state = pl.pallas_call(
         functools.partial(kernel, cfg),

time: 72.9 us -> 59.3 us (0.81)
  Pallas kernels: 67.4 us -> 53.7 us
    pallas_call x1, Pallas kernels: 67.4 us -> 53.7 us  [pair_call(): pl.pallas_call(functools.partial(pair_kernel, cfg), out_shape=(jax.ShapeD...]
where the time goes in v1:
time: 59.3 us; the launch traced here: 59.1 us
  Pallas kernels  53.7 us (91%)
  local copies, waits for them, and re-layouts  4.73 us (8%)
  between operations  0.65 us (1%)
    pallas_call x1, Pallas kernels, pair_call(): pl.pallas_call(functools.partial(pair_kernel, cfg), out_shape=(jax.ShapeD...  53.7 us
    unnamed x2, local copies, waits for them, and re-layouts  4.73 us

profile of v1, /device:TPU:0, one launch (start us, length us, event | category | flops | bytes accessed | tf_op | source)
XLA Modules:
  0.0 59.1 jit_solution(14556014410981930358)
XLA Ops:
  0.6 53.7 %shard_map.176 = (bf16[32,4,512]{2,1,0:T(4,128)(2,1)}, f32[2048,256]{1,0:T(8,128)}) custom-call(bf16[32,4,512]{2,1,0:T(4,128)(2,1)} %tok_hbm.1, f32[1,2048]{1,0:T(1,128)} %bitcast.14, bf16[512,256]{1,0:T(8,128)(2,1)} %wq_hbm.1, bf16[512,256]{1,0:T(8,128)(2,1)} %wk_hbm.1, bf16[512,256]{1,0:T(8,128)(2,1)} %wv_hbm.1, bf16[512,256]{1,0:T(8,128)(2,1)} %wg_hbm.1, ...), custom_call_target="tpu_custom_call" | custom-call | tf_op jit(solution)/shard_map/pallas_call | solution.py:989
  54.4 1.6 %copy.21 = bf16[32,4,512]{2,1,0:T(4,128)(2,1)} copy(bf16[32,4,512]{2,1,0:T(4,128)(2,1)} %get-tuple-element.8) | data formatting | bytes 262144
  56.0 3.1 %copy.22 = f32[32,64,256]{2,1,0:T(8,128)} copy(f32[32,64,256]{2,1,0:T(8,128)} %bitcast.11) | data formatting | bytes 4194304

commit v2 on v1

--- a/solution.py
+++ b/solution.py
@@ -480,10 +480,10 @@
     cfg,
     tok_hbm, gain_hbm, wq_hbm, wk_hbm, wv_hbm, wg_hbm, wb_hbm, wd_hbm, base_hbm, og_hbm, wo_hbm,
     state_hbm, pk_hbm, pv_hbm, pb_hbm, pd_hbm, acc_hbm,
-    mixed_ref, new_hbm,
-    gain_ref, wbd_ref, base_ref, og_ref, pk_ref, pv_ref, pb_ref, pd_ref, acc_ref, tok, wp, wo, st, normed, kq, res, tk, up, al, rows_a, rows_b, proj, own_part, part_send, part_recv, small_own, small_send, small_recv, send_buf, recv_buf, gate_buf, own_share,
-    in_sem, own_sem, wz_send, wz_recv, wy_send, wy_recv, t_send, f_send, t_recv, zr_send, zl_send, z_recv, y_send, y_recv, p_send, p_recv, r_send, r_recv,
-    out_sem, small_sem,
+    mixed_ref, st,
+    gain_ref, wbd_ref, base_ref, og_ref, pk_ref, pv_ref, pb_ref, pd_ref, acc_ref, tok, wp, wo, normed, kq, res, tk, up, al, rows_a, rows_b, proj, own_part, part_send, part_recv, small_own, small_send, small_recv, send_buf, recv_buf, gate_buf, own_share,
+    in_sem, own_sem, wz_send, wz_recv, wy_send, wy_recv, t_send, f_send, d_send, t_recv, zr_send, zl_send, z_recv, y_send, y_recv, p_send, p_recv, r_send, r_recv,
+    small_sem,
 ):
     n_grp, n_kv, n_tp, seqs, props, heads, hd = cfg
     width = heads * hd
@@ -549,33 +549,44 @@
         greet({"tp": lax.rem(t_me + d, n_tp)})
     greet({"grp": g_other})
     far_tp = 2 * (1 - chip) + core
-    greet({"kv": partner, "tp": far_tp})
-    pl.semaphore_wait(barrier, n_kv + n_tp)
+    pl.semaphore_wait(barrier, n_kv + n_tp - 1)
 
     def remote(src, dst, send, recv, dev):
         return pltpu.make_async_remote_copy(
             src, dst, send, recv, device_id=dev, device_id_type=MESH)
 
-    to_slot = core + 2 * home
-    to_kv = lax.rem(k + (1 - home) * (n_kv // 2), n_kv)
-    to_tp = 2 * chip + home * (1 - core) + (1 - home) * core
-
-    def tok_far():
-        return remote(tok.at[own_slot], tok.at[to_slot], t_send.at[0], t_recv.at[to_slot],
-                      {"kv": to_kv, "tp": far_tp})
-
-    def tok_near():
-        return remote(tok.at[own_slot], tok.at[to_slot], t_send.at[1], t_recv.at[to_slot],
-                      {"kv": to_kv, "tp": to_tp})
-
-    def tok_relay(j):
-        slot = 2 * j + core
-        return remote(tok.at[slot], tok.at[slot], f_send.at[j], t_recv.at[slot],
+    part = seqs // 2
+
+    def tok_piece(slot, half):
+        return tok.at[slot, pl.ds(half * part, part)]
+
+    def tok_partner(half):
+        return remote(tok_piece(own_slot, half), tok_piece(core, half), t_send.at[half],
+                      t_recv.at[core, half], {"kv": partner})
+
+    def tok_far(slot, half):
+        ref = tok_piece(slot, half)
+        return remote(ref, ref, f_send.at[slot // 2, half], t_recv.at[slot, half],
+                      {"tp": far_tp})
+
+    def tok_beside(slot, half):
+        ref = tok_piece(slot, half)
+        return remote(ref, ref, d_send.at[slot // 2, half], t_recv.at[slot, half],
                       {"tp": beside_core})
 
-    def tok_wait(slot):
-        remote(tok.at[slot], tok.at[slot], f_send.at[0], t_recv.at[slot],
+    def tok_wait(slot, half):
+        ref = tok_piece(slot, half)
+        remote(ref, ref, d_send.at[0, half], t_recv.at[slot, half],
                {"tp": beside_core}).wait_recv()
+
+    def tok_land(half):
+        tok_wait(core, half)
+
+        @pl.when(home == 1)
+        def _():
+            tok_far(core, half).start()
+
+        tok_beside(core, half).start()
 
     def w_slot(m, block, half):
         return wp.at[m, pl.ds(block * own_rows + half * piece, piece), :]
@@ -616,29 +627,47 @@
         ref = o_slot(origin, g_other)
         remote(ref, ref, y_send.at[origin], y_recv.at[origin], {"grp": g_other}).wait_recv()
 
-    def forward_step(s):
-        left = k - 1 - s
-        right = k + 1 + s
-
-        @pl.when(left >= 0)
-        def _():
-            z_right(left).wait_recv()
-
-            @pl.when(k < n_kv - 1)
-            def _():
-                z_right(left).start()
-
-            y_copy(left).start()
-
-        @pl.when(right < n_kv)
-        def _():
-            z_left(right).wait_recv()
-
-            @pl.when(k > 0)
-            def _():
-                z_left(right).start()
-
-            y_copy(right).start()
+    def from_left(origin):
+        z_right(origin).wait_recv()
+
+        @pl.when(k < n_kv - 1)
+        def _():
+            z_right(origin).start()
+
+        y_copy(origin).start()
+
+    def from_right(origin):
+        z_left(origin).wait_recv()
+
+        @pl.when(k > 0)
+        def _():
+            z_left(origin).start()
+
+        y_copy(origin).start()
+
+    def middle_pass(s):
+        @pl.when(jnp.logical_and(side == 1, pair == 0))
+        def _():
+            if s == 0:
+                from_left(k - 1)
+            else:
+                from_right(k + s)
+
+        @pl.when(jnp.logical_and(side == 0, pair == 1))
+        def _():
+            if s == 0:
+                from_right(k + 1)
+            else:
+                from_left(k - s)
+
+    def end_pass(s):
+        @pl.when(k == 0)
+        def _():
+            from_right(k + s)
+
+        @pl.when(k == n_kv - 1)
+        def _():
+            from_left(k - s)
 
     def p_copy(m):
         return remote(part_send.at[m], part_recv.at[m], p_send.at[m], p_recv.at[m],
@@ -648,21 +677,38 @@
         return remote(small_send, small_recv, p_send.at[n_src], p_recv.at[n_src],
                       {"kv": partner})
 
+    at_end = jnp.logical_or(k == 0, k == n_kv - 1)
     tok_in.wait()
-    tok_far().start()
-    tok_near().start()
-    for m in range(n_src):
+
+    @pl.when(home == 0)
+    def _():
+        for half in range(2):
+            tok_partner(half).start()
+
+    @pl.when(home == 1)
+    def _():
+        for half in range(2):
+            tok_far(2 + core, half).start()
+            tok_beside(2 + core, half).start()
+
+    def w_first(m):
         own_copies[m].wait()
         w_mate(m).start()
+
+    w_first(0)
+    w_first(1)
     own_copies[n_src].wait()
 
-    @pl.when(k < n_kv - 1)
+    @pl.when(k == 0)
     def _():
         z_right(k).start()
 
-    @pl.when(k > 0)
+    @pl.when(k == n_kv - 1)
     def _():
         z_left(k).start()
+
+    w_first(2)
+    w_first(3)
 
     blk = (
         lax.broadcasted_iota(jnp.int32, (width, width), 0) // hd
@@ -782,25 +828,43 @@
         st[where, :] = tile
         return carry
 
-    w_pass(0)
 
     @pl.when(home == 0)
     def _():
-        tok_wait(2 + core)
-        tok_relay(1).start()
-
-    lax.fori_loop(0, seqs // 2, renew, 0, unroll=2)
+        for half in range(2):
+            tok_wait(2 + core, half)
+            tok_beside(2 + core, half).start()
+
+    @pl.when(home == 1)
+    def _():
+        tok_land(0)
+
+    w_pass(0)
+
+    @pl.when(jnp.logical_not(at_end))
+    def _():
+        z_right(k).start()
+        z_left(k).start()
+
+    @pl.when(home == 1)
+    def _():
+        tok_land(1)
+
+    @pl.when(home == 0)
+    def _():
+        tok_land(0)
+
     w_pass(1)
-    tok_wait(core)
-    tok_relay(0).start()
-    lax.fori_loop(seqs // 2, seqs, renew, 0, unroll=2)
-    state_out = pltpu.make_async_copy(st, new_hbm, out_sem)
-    state_out.start()
+
+    @pl.when(home == 0)
+    def _():
+        tok_land(1)
+
     for copy in late:
         copy.wait()
-    w_pass(2)
-    tok_wait(1 - core)
-    tok_wait(3 - core)
+    for half in range(2):
+        tok_wait(3 - core, half)
+        tok_wait(1 - core, half)
     ones = jnp.ones((8, feats), BF16)
     squares = jnp.zeros((8, 2 * rows), F32)
     last = (((1,), (1,)), ((), ()))
@@ -827,13 +891,22 @@
         p_copy(m).start()
         own_part[m] = both[rows:]
 
-    for m in range(n_src):
-        w_ready(m)
-        project(m)
-        if m == 0:
-            w_pass(3)
-        else:
-            forward_step(m - 1)
+    w_ready(0)
+    project(0)
+    middle_pass(0)
+    w_pass(2)
+    w_ready(1)
+    project(1)
+    middle_pass(1)
+    w_pass(3)
+    w_ready(2)
+    project(2)
+    lax.fori_loop(0, seqs // 2, renew, 0, unroll=2)
+    w_ready(3)
+    project(3)
+    middle_pass(2)
+    end_pass(1)
+    lax.fori_loop(seqs // 2, seqs, renew, 0, unroll=2)
 
     pick = (
         lax.broadcasted_iota(jnp.int32, (all_heads, width), 0)
@@ -891,8 +964,10 @@
             send_buf[dest] = share.astype(BF16)
             r_copy(dest).start()
 
-    for m in range(3):
-        finish(m)
+    finish(0)
+    end_pass(2)
+    finish(1)
+    finish(2)
     keys = [rd(proj, pl.ds(t, seqs, stride=props), 0) for t in range(props)]
     queries = [rd(proj, pl.ds(t, seqs, stride=props), 1) for t in range(props)]
     values = [rd(proj, pl.ds(t, seqs, stride=props), 2) for t in range(props)]
@@ -913,6 +988,7 @@
         jnp.broadcast_to(og_ref[...], (8, hd)), tile_gain,
         precision=lax.Precision.HIGHEST, preferred_element_type=F32)[:1]
     wr(rows_a, every, out * gain)
+    end_pass(3)
     finish(n_src - 1)
     gate = rd(proj, every, 3)
     gate_buf[...] = (rd(rows_a, every) * (gate / (1.0 + jnp.exp(-gate)))).astype(BF16)
@@ -941,13 +1017,18 @@
         total = total + recv_buf[origin].astype(F32)
     mixed_ref[...] = total.reshape(seqs, props, feats).astype(BF16)
 
-    tok_far().wait_send()
-    tok_near().wait_send()
-    tok_relay(0).wait_send()
-
-    @pl.when(home == 0)
-    def _():
-        tok_relay(1).wait_send()
+    for half in range(2):
+        tok_beside(core, half).wait_send()
+        tok_beside(2 + core, half).wait_send()
+
+        @pl.when(home == 1)
+        def _():
+            tok_far(core, half).wait_send()
+            tok_far(2 + core, half).wait_send()
+
+        @pl.when(home == 0)
+        def _():
+            tok_partner(half).wait_send()
 
     for m in range(n_src):
         w_mate(m).wait_send()
@@ -973,7 +1054,6 @@
         return carry
 
     lax.fori_loop(0, n_kv, drain, 0)
-    state_out.wait()
 
 
 def pair_call(sizes, args, seqs, props, feats, heads, hd, width, rows, pad):
@@ -989,11 +1069,11 @@
     return pl.pallas_call(
         functools.partial(pair_kernel, cfg),
         out_shape=(
-            jax.ShapeDtypeStruct((seqs, props, feats), BF16),
-            jax.ShapeDtypeStruct((seqs * hd, width), F32),
+            pltpu.VMEM((seqs, props, feats), BF16),
+            pltpu.VMEM((seqs * hd, width), F32),
         ),
         in_specs=[hbm] * len(args),
-        out_specs=(vmem, pl.BlockSpec(memory_space=pl.ANY)),
+        out_specs=(vmem, vmem),
         scratch_shapes=[
             pltpu.VMEM((1, 2 * feats), F32),
             pltpu.VMEM((2 * all_heads, 2 * feats), BF16),
@@ -1001,7 +1081,6 @@
             pltpu.VMEM((5, seqs, props, feats), BF16),
             pltpu.VMEM((n_src, 2 * own_rows, width), BF16),
             pltpu.VMEM((n_tp, width, feats), BF16),
-            pltpu.VMEM((seqs * hd, width), F32),
             pltpu.VMEM((2 * rows, 2 * feats), BF16),
             pltpu.VMEM((width // 128, seqs * pad, 128), F32),
             pltpu.VMEM((width // 128, seqs * pad, 128), F32),
@@ -1025,18 +1104,18 @@
             dma((n_src + 1,)),
             *[dma((n_src,)) for _ in range(4)],
             dma((2,)),
-            dma((2,)),
-            dma((4,)),
+            dma((2, 2)),
+            dma((2, 2)),
+            dma((4, 2)),
             *[dma((n_kv,)) for _ in range(5)],
             dma((n_src + 1,)),
             dma((n_src + 1,)),
             dma((n_tp,)),
             dma((n_tp,)),
-            dma(()),
             dma((10,)),
         ],
         compiler_params=pltpu.CompilerParams(
-            collective_id=1, has_side_effects=True, vmem_limit_bytes=67043328),
+            collective_id=1, has_side_effects=True, vmem_limit_bytes=67043328 - rows * feats * 2 - seqs * hd * width * 4),
     )(*args)
 
 

time: 59.3 us -> 47.1 us (0.79)
  Pallas kernels: 53.7 us -> 44.3 us
  local copies, waits for them, and re-layouts: 4.73 us -> 1.98 us
    pallas_call x1, Pallas kernels: 53.7 us -> 44.3 us  [pair_call(): pl.pallas_call(functools.partial(pair_kernel, cfg), out_shape=(pltpu.VMEM...]
    unnamed x2, local copies, waits for them, and re-layouts: 4.73 us -> 1.98 us
where the time goes in v2:
time: 47.1 us; the launch traced here: 46.9 us
  Pallas kernels  44.3 us (94%)
  local copies, waits for them, and re-layouts  1.98 us (4%)
  between operations  0.65 us (1%)
    pallas_call x1, Pallas kernels, pair_call(): pl.pallas_call(functools.partial(pair_kernel, cfg), out_shape=(pltpu.VMEM...  44.3 us
    unnamed x2, local copies, waits for them, and re-layouts  1.98 us

profile of v2, /device:TPU:0, one launch (start us, length us, event | category | flops | bytes accessed | tf_op | source)
XLA Modules:
  0.0 46.9 jit_solution(16006057563020984684)
XLA Ops:
  0.6 44.3 %shard_map.176 = (bf16[32,4,512]{2,1,0:T(4,128)(2,1)S(1)}, f32[2048,256]{1,0:T(8,128)S(1)}) custom-call(bf16[32,4,512]{2,1,0:T(4,128)(2,1)} %tok_hbm.1, f32[1,2048]{1,0:T(1,128)} %bitcast.14, bf16[512,256]{1,0:T(8,128)(2,1)} %wq_hbm.1, bf16[512,256]{1,0:T(8,128)(2,1)} %wk_hbm.1, bf16[512,256]{1,0:T(8,128)(2,1)} %wv_hbm.1, bf16[512,256]{1,0:T(8,128)(2,1)} %wg_hbm.1, ...), custom_call_target="tpu_custom_call" | custom-call | tf_op jit(solution)/shard_map/pallas_call | solution.py:1069
  45.0 0.7 %copy.21 = bf16[32,4,512]{2,1,0:T(4,128)(2,1)} copy(bf16[32,4,512]{2,1,0:T(4,128)(2,1)S(1)} %get-tuple-element.6) | data formatting | bytes 262144
  45.6 1.3 %copy.22 = f32[32,64,256]{2,1,0:T(8,128)} copy(f32[32,64,256]{2,1,0:T(8,128)S(1)} %bitcast.10) | data formatting | bytes 4194304

commit v3 on v2

--- a/solution.py
+++ b/solution.py
@@ -494,6 +494,9 @@
     own_rows = wk_hbm.shape[0]
     piece = own_rows // n_grp
     out_piece = wo.shape[1] // n_grp
+    out_bits = 2
+    w_bits = 2
+    out_bit = out_piece // out_bits
     feats = tok_hbm.shape[2]
     sources = [wk_hbm, wq_hbm, wv_hbm, wg_hbm]
     n_src = len(sources)
@@ -560,9 +563,17 @@
     def tok_piece(slot, half):
         return tok.at[slot, pl.ds(half * part, part)]
 
-    def tok_partner(half):
-        return remote(tok_piece(own_slot, half), tok_piece(core, half), t_send.at[half],
-                      t_recv.at[core, half], {"kv": partner})
+    def tok_partner():
+        return remote(tok_piece(4, 0), tok_piece(core, 0), t_send.at[0],
+                      t_recv.at[core, 0], {"kv": partner})
+
+    def tok_shift():
+        return remote(tok_piece(4, 1), tok_piece(5, 1), t_send.at[1], t_recv.at[4, 1],
+                      {"tp": far_tp})
+
+    def tok_relay():
+        return remote(tok_piece(5, 1), tok_piece(core, 1), t_send.at[0],
+                      t_recv.at[core, 1], {"kv": partner})
 
     def tok_far(slot, half):
         ref = tok_piece(slot, half)
@@ -579,71 +590,86 @@
         remote(ref, ref, d_send.at[0, half], t_recv.at[slot, half],
                {"tp": beside_core}).wait_recv()
 
-    def tok_land(half):
-        tok_wait(core, half)
-
-        @pl.when(home == 1)
-        def _():
-            tok_far(core, half).start()
-
-        tok_beside(core, half).start()
-
-    def w_slot(m, block, half):
-        return wp.at[m, pl.ds(block * own_rows + half * piece, piece), :]
-
-    def w_mate(m):
-        ref = w_slot(m, side, g)
-        return remote(ref, ref, wz_send.at[m], wz_recv.at[m], {"kv": mate})
-
-    def w_share(m):
-        ref = w_slot(m, 1 - side, g)
-        return remote(ref, ref, wy_send.at[m], wy_recv.at[m], {"grp": g_other})
+    def tok_land_z():
+        tok_wait(core, 1 - home)
+        tok_far(core, 1 - home).start()
+        tok_beside(core, 1 - home).start()
+
+    def tok_land_x():
+        tok_wait(core, home)
+        tok_beside(core, home).start()
+
+    def w_slot(m, block, half, bit):
+        at = pl.ds(block * own_rows + half * piece + bit * (piece // w_bits), piece // w_bits)
+        return wp.at[m, at, :]
+
+    def w_mate(m, bit):
+        ref = w_slot(m, side, g, bit)
+        return remote(ref, ref, wz_send.at[m, bit], wz_recv.at[m, bit], {"kv": mate})
+
+    def w_share(m, bit):
+        ref = w_slot(m, 1 - side, g, bit)
+        return remote(ref, ref, wy_send.at[m, bit], wy_recv.at[m, bit], {"grp": g_other})
 
     def w_pass(m):
-        ref = w_slot(m, 1 - side, g)
-        remote(ref, ref, wz_send.at[m], wz_recv.at[m], {"kv": mate}).wait_recv()
-        w_share(m).start()
+        for bit in range(w_bits):
+            ref = w_slot(m, 1 - side, g, bit)
+            remote(ref, ref, wz_send.at[m, bit], wz_recv.at[m, bit], {"kv": mate}).wait_recv()
+            w_share(m, bit).start()
 
     def w_ready(m):
-        ref = w_slot(m, 1 - side, g_other)
-        remote(ref, ref, wy_send.at[m], wy_recv.at[m], {"grp": g_other}).wait_recv()
-
-    def o_slot(origin, part):
-        return wo.at[origin, pl.ds(part * out_piece, out_piece), :]
-
-    def z_right(origin):
-        ref = o_slot(origin, g)
-        return remote(ref, ref, zr_send.at[origin], z_recv.at[origin], {"kv": k + 1})
-
-    def z_left(origin):
-        ref = o_slot(origin, g)
-        return remote(ref, ref, zl_send.at[origin], z_recv.at[origin], {"kv": k - 1})
-
-    def y_copy(origin):
-        ref = o_slot(origin, g)
-        return remote(ref, ref, y_send.at[origin], y_recv.at[origin], {"grp": g_other})
+        for bit in range(w_bits):
+            ref = w_slot(m, 1 - side, g_other, bit)
+            remote(ref, ref, wy_send.at[m, bit], wy_recv.at[m, bit], {"grp": g_other}).wait_recv()
+
+    def o_slot(origin, part, bit):
+        return wo.at[origin, pl.ds(part * out_piece + bit * out_bit, out_bit), :]
+
+    def z_right(origin, bit):
+        ref = o_slot(origin, g, bit)
+        return remote(ref, ref, zr_send.at[origin, bit], z_recv.at[origin, bit], {"kv": k + 1})
+
+    def z_left(origin, bit):
+        ref = o_slot(origin, g, bit)
+        return remote(ref, ref, zl_send.at[origin, bit], z_recv.at[origin, bit], {"kv": k - 1})
+
+    def y_copy(origin, bit):
+        ref = o_slot(origin, g, bit)
+        return remote(ref, ref, y_send.at[origin, bit], y_recv.at[origin, bit], {"grp": g_other})
 
     def y_wait(origin):
-        ref = o_slot(origin, g_other)
-        remote(ref, ref, y_send.at[origin], y_recv.at[origin], {"grp": g_other}).wait_recv()
+        for bit in range(out_bits):
+            ref = o_slot(origin, g_other, bit)
+            remote(ref, ref, y_send.at[origin, bit], y_recv.at[origin, bit],
+                   {"grp": g_other}).wait_recv()
+
+    def right_start(origin):
+        for bit in range(out_bits):
+            z_right(origin, bit).start()
+
+    def left_start(origin):
+        for bit in range(out_bits):
+            z_left(origin, bit).start()
 
     def from_left(origin):
-        z_right(origin).wait_recv()
-
-        @pl.when(k < n_kv - 1)
-        def _():
-            z_right(origin).start()
-
-        y_copy(origin).start()
+        for bit in range(out_bits):
+            z_right(origin, bit).wait_recv()
+
+            @pl.when(k < n_kv - 1)
+            def _():
+                z_right(origin, bit).start()
 
     def from_right(origin):
-        z_left(origin).wait_recv()
-
-        @pl.when(k > 0)
-        def _():
-            z_left(origin).start()
-
-        y_copy(origin).start()
+        for bit in range(out_bits):
+            z_left(origin, bit).wait_recv()
+
+            @pl.when(k > 0)
+            def _():
+                z_left(origin, bit).start()
+
+    def share_out(origin):
+        for bit in range(out_bits):
+            y_copy(origin, bit).start()
 
     def middle_pass(s):
         @pl.when(jnp.logical_and(side == 1, pair == 0))
@@ -660,21 +686,33 @@
             else:
                 from_left(k - s)
 
+    def middle_share(s):
+        @pl.when(jnp.logical_and(side == 1, pair == 0))
+        def _():
+            share_out(k - 1 if s == 0 else k + s)
+
+        @pl.when(jnp.logical_and(side == 0, pair == 1))
+        def _():
+            share_out(k + 1 if s == 0 else k - s)
+
     def end_pass(s):
         @pl.when(k == 0)
         def _():
             from_right(k + s)
+            share_out(k + s)
 
         @pl.when(k == n_kv - 1)
         def _():
             from_left(k - s)
-
-    def p_copy(m):
-        return remote(part_send.at[m], part_recv.at[m], p_send.at[m], p_recv.at[m],
-                      {"kv": partner})
+            share_out(k - s)
+
+    def p_copy(m, b):
+        at = pl.ds(b * half_rows, half_rows)
+        return remote(part_send.at[m, at], part_recv.at[m, at], p_send.at[m, b],
+                      p_recv.at[m, b], {"kv": partner})
 
     def small_copy():
-        return remote(small_send, small_recv, p_send.at[n_src], p_recv.at[n_src],
+        return remote(small_send, small_recv, p_send.at[n_src, 0], p_recv.at[n_src, 0],
                       {"kv": partner})
 
     at_end = jnp.logical_or(k == 0, k == n_kv - 1)
@@ -682,8 +720,8 @@
 
     @pl.when(home == 0)
     def _():
-        for half in range(2):
-            tok_partner(half).start()
+        tok_shift().start()
+        tok_partner().start()
 
     @pl.when(home == 1)
     def _():
@@ -693,22 +731,30 @@
 
     def w_first(m):
         own_copies[m].wait()
-        w_mate(m).start()
+        for bit in range(w_bits):
+            w_mate(m, bit).start()
 
     w_first(0)
-    w_first(1)
     own_copies[n_src].wait()
 
-    @pl.when(k == 0)
+    def w_rest():
+        @pl.when(k == 0)
+        def _():
+            right_start(k)
+
+        @pl.when(k == n_kv - 1)
+        def _():
+            left_start(k)
+
+        w_first(1)
+        w_first(2)
+        w_first(3)
+
+    relays_first = jnp.logical_and(at_end, home == 1)
+
+    @pl.when(jnp.logical_not(relays_first))
     def _():
-        z_right(k).start()
-
-    @pl.when(k == n_kv - 1)
-    def _():
-        z_left(k).start()
-
-    w_first(2)
-    w_first(3)
+        w_rest()
 
     blk = (
         lax.broadcasted_iota(jnp.int32, (width, width), 0) // hd
@@ -734,18 +780,34 @@
             ref[(*lead, c, at)] = x[:, c * lanes : (c + 1) * lanes]
 
     every = pl.ds(0, rows)
+    count = seqs // 2
+    half_rows = count * props
 
     pad = 2 * props
 
+    def head_first(x, head):
+        block, at = divmod(head * hd, lanes)
+        x = x[:, block * lanes : (block + 1) * lanes]
+        return jnp.concatenate([x[:, at:], x[:, :at]], axis=-1) if at else x
+
+    def put_heads(ref, x, first, each, low=0):
+        step = heads * each
+        for head in range(heads):
+            at = pl.ds(low * step + head * each + first, x.shape[0], stride=step)
+            ref[at] = head_first(x, head)
+
     def by_state(s, carry):
-        tile = st[pl.ds(pl.multiple_of(s * hd, hd), hd), :]
-        stacked = jnp.concatenate([(tile * mask).astype(BF16) for mask in masks], axis=0)
-        at = pl.ds(pl.multiple_of(s * pad, pad), pad)
-        lhs = rd(kq, at).astype(BF16)
-        wr(res, at, jnp.dot(lhs, stacked, preferred_element_type=F32))
+        at = pl.ds(pl.multiple_of(s * heads * pad, heads * pad), heads * pad)
+        tile = st[pl.ds(pl.multiple_of(s * hd, hd), hd), :].astype(BF16)
+        found = jnp.dot(kq[at, :hd].astype(BF16), tile, preferred_element_type=F32)
+        own = masks[0] * found[:pad]
+        for head in range(1, heads):
+            own = own + masks[head] * found[head * pad : (head + 1) * pad]
+        wr(res, pl.ds(pl.multiple_of(s * pad, pad), pad), own)
         return carry
 
-    def solve(keys, values, weights, logs, queries):
+    def solve(keys, values, weights, logs, queries, start=0):
+        count = keys[0].shape[0]
         cumul = []
         run = None
         for t in range(props):
@@ -758,14 +820,14 @@
             full = [(i, j) for i in range(props) for j in range(i + 1)]
             products += [queries[i] * keys[j] for i, j in full]
         sums = head_sum(jnp.concatenate(products, axis=0))
-        sums = [sums[i * seqs : (i + 1) * seqs] for i in range(len(products))]
+        sums = [sums[i * count : (i + 1) * count] for i in range(len(products))]
         kk = dict(zip(low, sums))
         qk = dict(zip(full, sums[len(low):]))
         dec = {pair: jnp.exp(cumul[pair[0]] - cumul[pair[1]]) for pair in low}
         growth = [jnp.exp(c) for c in cumul]
         update = []
         for t in range(props):
-            seen = rd(res, pl.ds(t, seqs, stride=pad))
+            seen = rd(res, pl.ds(start * pad + t, count, stride=pad))
             term = values[t] - growth[t] * seen
             for j in range(t):
                 term = term - kk[t, j] * dec[t, j] * update[j]
@@ -773,7 +835,8 @@
         outs = []
         if queries is not None:
             for t in range(props):
-                out = growth[t] * rd(res, pl.ds(props + t, seqs, stride=pad))
+                out = growth[t] * rd(
+                    res, pl.ds(start * pad + props + t, count, stride=pad))
                 for j in range(t + 1):
                     score = qk[t, j] if j == t else qk[t, j] * dec[t, j]
                     out = out + score * update[j]
@@ -805,29 +868,36 @@
         live = (acc_ref[...] > t).astype(F32)
         weights.append(over_lanes(jax.nn.sigmoid(pb_ref[t]) * live))
         logs.append(over_lanes(pd_ref[t] * live))
-        wr(kq, pl.ds(t, seqs, stride=pad), keys[t])
-        wr(kq, pl.ds(props + t, seqs, stride=pad), keys[t])
+        put_heads(kq, keys[t], t, pad)
+        put_heads(kq, keys[t], props + t, pad)
     state_in.wait()
     lax.fori_loop(0, seqs, by_state, 0, unroll=4)
     cumul, growth, update, _ = solve(keys, values, weights, logs, None)
     al[...] = growth[-1]
     for t in range(props):
-        wr(tk, pl.ds(t, seqs, stride=pad), jnp.exp(cumul[-1] - cumul[t]) * keys[t])
-        wr(up, pl.ds(t, seqs, stride=pad), update[t])
-        wr(tk, pl.ds(props + t, seqs, stride=pad), jnp.zeros((seqs, width), F32))
-        wr(up, pl.ds(props + t, seqs, stride=pad), jnp.zeros((seqs, width), F32))
+        put_heads(tk, jnp.exp(cumul[-1] - cumul[t]) * keys[t], t, props)
+        for head in range(heads):
+            wr(up, pl.ds(head * props + t, seqs, stride=heads * props), masks[head] * update[t])
 
     def renew(s, carry):
-        at = pl.ds(pl.multiple_of(s * pad, pad), pad)
+        each = heads * props
+        at = pl.ds(pl.multiple_of(s * each, each), each)
         outer = lax.dot_general(
-            rd(tk, at), rd(up, at), (((0,), (0,)), ((), ())), preferred_element_type=F32)
+            tk[at, :hd], rd(up, at), (((0,), (0,)), ((), ())), preferred_element_type=F32)
         where = pl.ds(pl.multiple_of(s * hd, hd), hd)
-        tile = al[pl.ds(s, 1), :] * st[where, :]
-        for h in range(heads):
-            tile = tile + masks[h] * outer[h * hd : (h + 1) * hd, :]
-        st[where, :] = tile
+        st[where, :] = al[pl.ds(s, 1), :] * st[where, :] + outer
         return carry
 
+
+    @pl.when(home == 1)
+    def _():
+        remote(tok_piece(5, 1), tok_piece(5, 1), t_send.at[1], t_recv.at[4, 1],
+               {"tp": far_tp}).wait_recv()
+        tok_relay().start()
+
+    @pl.when(relays_first)
+    def _():
+        w_rest()
 
     @pl.when(home == 0)
     def _():
@@ -837,28 +907,29 @@
 
     @pl.when(home == 1)
     def _():
-        tok_land(0)
+        tok_land_z()
 
     w_pass(0)
 
     @pl.when(jnp.logical_not(at_end))
     def _():
-        z_right(k).start()
-        z_left(k).start()
+        right_start(k)
+        left_start(k)
+
+    @pl.when(home == 0)
+    def _():
+        tok_land_z()
+        tok_land_x()
+
+    middle_pass(0)
+    middle_share(0)
 
     @pl.when(home == 1)
     def _():
-        tok_land(1)
-
-    @pl.when(home == 0)
-    def _():
-        tok_land(0)
+        tok_land_x()
 
     w_pass(1)
-
-    @pl.when(home == 0)
-    def _():
-        tok_land(1)
+    middle_pass(1)
 
     for copy in late:
         copy.wait()
@@ -881,6 +952,15 @@
         squares = squares + lax.dot_general(ones, lo, last, preferred_element_type=F32)
     raw = lax.dot_general(wbd_ref[...], normed[...], last, preferred_element_type=F32)
     small = jnp.concatenate([raw, squares], axis=0)
+    kind = lax.broadcasted_iota(jnp.int32, (small_own.shape[0], small.shape[0]), 0)
+    taken = lax.broadcasted_iota(jnp.int32, (small_own.shape[0], small.shape[0]), 1)
+    first_head = t_me * heads
+    wanted = jnp.where(
+        kind < heads, first_head + kind,
+        jnp.where(kind < 2 * heads, all_heads + first_head + kind - heads, 2 * all_heads))
+    small = jnp.dot(
+        (taken == wanted).astype(F32), small,
+        precision=lax.Precision.HIGHEST, preferred_element_type=F32)
     small_send[...] = small[:, :rows]
     small_copy().start()
     small_own[...] = small[:, rows:]
@@ -888,98 +968,86 @@
     def project(m):
         both = jnp.dot(normed[...], wp[m], preferred_element_type=F32)
         part_send[m] = both[:rows].astype(BF16)
-        p_copy(m).start()
         own_part[m] = both[rows:]
+
+    def give(*pieces):
+        for m, b in pieces:
+            p_copy(m, b).start()
 
     w_ready(0)
     project(0)
-    middle_pass(0)
+    give((0, 0), (0, 1))
     w_pass(2)
     w_ready(1)
     project(1)
-    middle_pass(1)
+    give((1, 0))
+    middle_pass(2)
     w_pass(3)
+    end_pass(1)
+    middle_share(1)
+    middle_share(2)
     w_ready(2)
     project(2)
-    lax.fori_loop(0, seqs // 2, renew, 0, unroll=2)
+    give((2, 0), (1, 1))
+    lax.fori_loop(0, seqs // 2, renew, 0, unroll=4)
     w_ready(3)
     project(3)
-    middle_pass(2)
-    end_pass(1)
-    lax.fori_loop(seqs // 2, seqs, renew, 0, unroll=2)
-
-    pick = (
-        lax.broadcasted_iota(jnp.int32, (all_heads, width), 0)
-        == t_me * heads + lax.broadcasted_iota(jnp.int32, (all_heads, width), 1) // hd
-    ).astype(F32)
+    give((3, 0), (2, 1), (3, 1))
+    end_pass(2)
+    lax.fori_loop(seqs // 2, seqs, renew, 0, unroll=4)
+
     small_copy().wait_recv()
     small = small_own[...] + small_recv[...]
-    scale = lax.rsqrt(small[2 * all_heads :] / (n_tp * feats) + EPS)
-    beta = small[:all_heads] * scale[:1]
-    decay = small[all_heads : 2 * all_heads] * scale[:1]
+    scale = lax.rsqrt(small[2 * heads :] / (n_tp * feats) + EPS)
+    beta = small[:heads] * scale[:1]
+    decay = small[heads : 2 * heads] * scale[:1]
 
     def spread(x, over):
         return lax.dot_general(
             x, over, (((0,), (0,)), ((), ())),
             precision=lax.Precision.HIGHEST, preferred_element_type=F32)
 
-    wr(rows_a, every, spread(jax.nn.sigmoid(beta), pick))
-    weights = split(rows_a)
+    wr(rows_a, every, spread(jax.nn.sigmoid(beta), own_head))
     base = jnp.zeros((1, width), F32)
     for h in range(heads):
         base = jnp.where(lane_head == h, base_ref[:, h : h + 1], base)
-    wr(rows_b, every, -base * spread(jax.nn.softplus(decay), pick))
-    logs = split(rows_b)
+    wr(rows_b, every, -base * spread(jax.nn.softplus(decay), own_head))
     row_scale = spread(
-        scale, (lax.broadcasted_iota(jnp.int32, (8, width), 0) == 0).astype(F32))
-
-    def finish(m):
-        p_copy(m).wait_recv()
-        value = (own_part[m] + part_recv[m].astype(F32)) * row_scale
+        scale, (lax.broadcasted_iota(jnp.int32, (scale.shape[0], width), 0) == 0).astype(F32))
+
+    def finish(m, b):
+        p_copy(m, b).wait_recv()
+        at = slice(b * half_rows, (b + 1) * half_rows)
+        value = (own_part[m, at] + part_recv[m, at].astype(F32)) * row_scale[at]
         if m == 0:
             value = value * lax.rsqrt(head_sum(value * value) + EPS)
         elif m == 1:
             value = value * lax.rsqrt(head_sum(value * value) + EPS) * hd ** (-0.5)
-        wr(proj, every, value, m)
-
-    def r_copy(dest):
-        return pltpu.make_async_remote_copy(
-            send_buf.at[dest], recv_buf.at[t_me], r_send.at[dest], r_recv.at[t_me],
-            device_id={"tp": dest}, device_id_type=MESH)
-
-    def r_wait(origin):
-        pltpu.make_async_remote_copy(
-            send_buf.at[origin], recv_buf.at[origin], r_send.at[origin], r_recv.at[origin],
-            device_id={"tp": origin}, device_id_type=MESH).wait_recv()
-
-    def send_share(dest):
-        share = jnp.dot(gate_buf[...], wo[dest], preferred_element_type=F32)
+        wr(proj, pl.ds(b * half_rows, half_rows), value, m)
+
+    def r_copy(dest, b):
+        at = pl.ds(b * half_rows, half_rows)
+        return remote(send_buf.at[dest, at], recv_buf.at[t_me, at], r_send.at[dest, b],
+                      r_recv.at[t_me, b], {"tp": dest})
+
+    def r_wait(origin, b):
+        at = pl.ds(b * half_rows, half_rows)
+        remote(send_buf.at[origin, at], recv_buf.at[origin, at], r_send.at[origin, b],
+               r_recv.at[origin, b], {"tp": origin}).wait_recv()
+
+    def send_share(dest, b):
+        at = slice(b * half_rows, (b + 1) * half_rows)
+        share = jnp.dot(gate_buf[at], wo[dest], preferred_element_type=F32)
 
         @pl.when(dest == t_me)
         def _():
-            own_share[...] = share
+            own_share[at] = share
 
         @pl.when(dest != t_me)
         def _():
-            send_buf[dest] = share.astype(BF16)
-            r_copy(dest).start()
-
-    finish(0)
-    end_pass(2)
-    finish(1)
-    finish(2)
-    keys = [rd(proj, pl.ds(t, seqs, stride=props), 0) for t in range(props)]
-    queries = [rd(proj, pl.ds(t, seqs, stride=props), 1) for t in range(props)]
-    values = [rd(proj, pl.ds(t, seqs, stride=props), 2) for t in range(props)]
-    for t in range(props):
-        wr(kq, pl.ds(t, seqs, stride=pad), keys[t])
-        wr(kq, pl.ds(props + t, seqs, stride=pad), queries[t])
-    lax.fori_loop(0, seqs, by_state, 0, unroll=4)
-    outs = solve(keys, values, weights, logs, queries)[3]
-    for t in range(props):
-        wr(rows_a, pl.ds(t, seqs, stride=props), outs[t])
-    out = rd(rows_a, every)
-    out = out * lax.rsqrt(head_sum(out * out) / hd + EPS)
+            send_buf[dest, at] = share.astype(BF16)
+            r_copy(dest, b).start()
+
     tile_gain = (
         lax.broadcasted_iota(jnp.int32, (hd, width), 0)
         == lax.broadcasted_iota(jnp.int32, (hd, width), 1) % hd
@@ -987,69 +1055,111 @@
     gain = jnp.dot(
         jnp.broadcast_to(og_ref[...], (8, hd)), tile_gain,
         precision=lax.Precision.HIGHEST, preferred_element_type=F32)[:1]
-    wr(rows_a, every, out * gain)
+
+    def delta(b):
+        low, first = b * count, b * half_rows
+        steps = [pl.ds(first + t, count, stride=props) for t in range(props)]
+        for m in range(3):
+            finish(m, b)
+        keys, queries, values = [[rd(proj, at, m) for at in steps] for m in range(3)]
+        weights = [rd(rows_a, at) for at in steps]
+        logs = [rd(rows_b, at) for at in steps]
+        for t in range(props):
+            put_heads(kq, keys[t], t, pad, low)
+            put_heads(kq, queries[t], props + t, pad, low)
+        lax.fori_loop(low, low + count, by_state, 0, unroll=4)
+        outs = solve(keys, values, weights, logs, queries, low)[3]
+        for t in range(props):
+            wr(rows_a, steps[t], outs[t])
+        half = pl.ds(first, half_rows)
+        out = rd(rows_a, half)
+        out = out * lax.rsqrt(head_sum(out * out) / hd + EPS) * gain
+        finish(n_src - 1, b)
+        gate = rd(proj, half, 3)
+        gate_buf[first : first + half_rows] = (
+            out * (gate / (1.0 + jnp.exp(-gate)))).astype(BF16)
+
+    def take(b):
+        def step(s, carry):
+            @pl.when(k - s >= 0)
+            def _():
+                if b == 0:
+                    @pl.when(s > 0)
+                    def _():
+                        y_wait(k - s)
+
+                send_share(k - s, b)
+
+            @pl.when(jnp.logical_and(s > 0, k + s < n_kv))
+            def _():
+                if b == 0:
+                    y_wait(k + s)
+                send_share(k + s, b)
+
+            return carry
+
+        return step
+
+    def settle(b):
+        at = slice(b * half_rows, (b + 1) * half_rows)
+        total = own_share[at]
+        for d in range(1, n_tp):
+            origin = lax.rem(t_me + d, n_tp)
+            r_wait(origin, b)
+            total = total + recv_buf[origin, at].astype(F32)
+        mixed_ref[b * count : (b + 1) * count] = total.reshape(count, props, feats).astype(BF16)
+
+    delta(0)
     end_pass(3)
-    finish(n_src - 1)
-    gate = rd(proj, every, 3)
-    gate_buf[...] = (rd(rows_a, every) * (gate / (1.0 + jnp.exp(-gate)))).astype(BF16)
-
-    def take(s, carry):
-        @pl.when(k - s >= 0)
-        def _():
-            @pl.when(s > 0)
-            def _():
-                y_wait(k - s)
-
-            send_share(k - s)
-
-        @pl.when(jnp.logical_and(s > 0, k + s < n_kv))
-        def _():
-            y_wait(k + s)
-            send_share(k + s)
-
-        return carry
-
-    lax.fori_loop(0, n_kv, take, 0)
-    total = own_share[...]
-    for d in range(1, n_tp):
-        origin = lax.rem(t_me + d, n_tp)
-        r_wait(origin)
-        total = total + recv_buf[origin].astype(F32)
-    mixed_ref[...] = total.reshape(seqs, props, feats).astype(BF16)
+    lax.fori_loop(0, n_kv // 2, take(0), 0)
+    delta(1)
+    lax.fori_loop(n_kv // 2, n_kv - 1, take(0), 0)
+    lax.fori_loop(0, n_kv - 1, take(1), 0)
+    lax.fori_loop(n_kv - 1, n_kv, take(0), 0)
+    lax.fori_loop(n_kv - 1, n_kv, take(1), 0)
+    settle(0)
+    settle(1)
 
     for half in range(2):
         tok_beside(core, half).wait_send()
         tok_beside(2 + core, half).wait_send()
-
-        @pl.when(home == 1)
-        def _():
-            tok_far(core, half).wait_send()
-            tok_far(2 + core, half).wait_send()
-
-        @pl.when(home == 0)
-        def _():
-            tok_partner(half).wait_send()
+    tok_far(core, 1 - home).wait_send()
+
+    @pl.when(home == 1)
+    def _():
+        tok_far(2 + core, 0).wait_send()
+        tok_far(2 + core, 1).wait_send()
+        tok_relay().wait_send()
+
+    @pl.when(home == 0)
+    def _():
+        tok_partner().wait_send()
+        tok_shift().wait_send()
 
     for m in range(n_src):
-        w_mate(m).wait_send()
-        w_share(m).wait_send()
-        p_copy(m).wait_send()
+        for bit in range(w_bits):
+            w_mate(m, bit).wait_send()
+            w_share(m, bit).wait_send()
+        p_copy(m, 0).wait_send()
+        p_copy(m, 1).wait_send()
     small_copy().wait_send()
     for d in range(1, n_tp):
-        r_copy(lax.rem(t_me + d, n_tp)).wait_send()
+        r_copy(lax.rem(t_me + d, n_tp), 0).wait_send()
+        r_copy(lax.rem(t_me + d, n_tp), 1).wait_send()
 
     def drain(o, carry):
-        @pl.when(jnp.logical_and(o <= k, k < n_kv - 1))
-        def _():
-            z_right(o).wait_send()
-
-        @pl.when(jnp.logical_and(o >= k, k > 0))
-        def _():
-            z_left(o).wait_send()
-
-        @pl.when(o != k)
-        def _():
-            y_copy(o).wait_send()
+        for bit in range(out_bits):
+            @pl.when(jnp.logical_and(o <= k, k < n_kv - 1))
+            def _():
+                z_right(o, bit).wait_send()
+
+            @pl.when(jnp.logical_and(o >= k, k > 0))
+            def _():
+                z_left(o, bit).wait_send()
+
+            @pl.when(o != k)
+            def _():
+                y_copy(o, bit).wait_send()
 
         return carry
 
@@ -1065,7 +1175,7 @@
     own_rows = args[2].shape[0]
     all_heads = args[6].shape[0]
     n_src = 4
-    small = (2 * all_heads + 8, rows)
+    small = (2 * heads + 8, rows)
     return pl.pallas_call(
         functools.partial(pair_kernel, cfg),
         out_shape=(
@@ -1078,14 +1188,14 @@
             pltpu.VMEM((1, 2 * feats), F32),
             pltpu.VMEM((2 * all_heads, 2 * feats), BF16),
             *[pltpu.VMEM(args[i].shape, args[i].dtype) for i in (8, 9, 12, 13, 14, 15, 16)],
-            pltpu.VMEM((5, seqs, props, feats), BF16),
+            pltpu.VMEM((6, seqs, props, feats), BF16),
             pltpu.VMEM((n_src, 2 * own_rows, width), BF16),
             pltpu.VMEM((n_tp, width, feats), BF16),
             pltpu.VMEM((2 * rows, 2 * feats), BF16),
+            pltpu.VMEM((seqs * heads * pad, 128), F32),
             pltpu.VMEM((width // 128, seqs * pad, 128), F32),
-            pltpu.VMEM((width // 128, seqs * pad, 128), F32),
-            pltpu.VMEM((width // 128, seqs * pad, 128), F32),
-            pltpu.VMEM((width // 128, seqs * pad, 128), F32),
+            pltpu.VMEM((seqs * heads * props, 128), F32),
+            pltpu.VMEM((width // 128, seqs * heads * props, 128), F32),
             pltpu.VMEM((seqs, width), F32),
             pltpu.VMEM((width // 128, rows, 128), F32),
             pltpu.VMEM((width // 128, rows, 128), F32),
@@ -1102,16 +1212,16 @@
             pltpu.VMEM((rows, feats), F32),
             dma((2,)),
             dma((n_src + 1,)),
-            *[dma((n_src,)) for _ in range(4)],
+            *[dma((n_src, 2)) for _ in range(4)],
             dma((2,)),
             dma((2, 2)),
             dma((2, 2)),
-            dma((4, 2)),
-            *[dma((n_kv,)) for _ in range(5)],
-            dma((n_src + 1,)),
-            dma((n_src + 1,)),
-            dma((n_tp,)),
-            dma((n_tp,)),
+            dma((5, 2)),
+            *[dma((n_kv, 2)) for _ in range(5)],
+            dma((n_src + 1, 2)),
+            dma((n_src + 1, 2)),
+            dma((n_tp, 2)),
+            dma((n_tp, 2)),
             dma((10,)),
         ],
         compiler_params=pltpu.CompilerParams(

time: 47.1 us -> 44.2 us (0.938)
  Pallas kernels: 44.3 us -> 41.5 us
    pallas_call x1, Pallas kernels: 44.3 us -> 41.5 us  [pair_call(): pl.pallas_call(functools.partial(pair_kernel, cfg), out_shape=(pltpu.VMEM...]
where the time goes in v3:
time: 44.2 us; the launch traced here: 44.1 us
  Pallas kernels  41.5 us (94%)
  local copies, waits for them, and re-layouts  1.98 us (4%)
  between operations  0.65 us (1%)
    pallas_call x1, Pallas kernels, pair_call(): pl.pallas_call(functools.partial(pair_kernel, cfg), out_shape=(pltpu.VMEM...  41.5 us
    unnamed x2, local copies, waits for them, and re-layouts  1.98 us

profile of v3, /device:TPU:0, one launch (start us, length us, event | category | flops | bytes accessed | tf_op | source)
XLA Modules:
  0.0 44.1 jit_solution(4653145499448130701)
XLA Ops:
  0.6 41.5 %shard_map.176 = (bf16[32,4,512]{2,1,0:T(4,128)(2,1)S(1)}, f32[2048,256]{1,0:T(8,128)S(1)}) custom-call(bf16[32,4,512]{2,1,0:T(4,128)(2,1)} %tok_hbm.1, f32[1,2048]{1,0:T(1,128)} %bitcast.14, bf16[512,256]{1,0:T(8,128)(2,1)} %wq_hbm.1, bf16[512,256]{1,0:T(8,128)(2,1)} %wk_hbm.1, bf16[512,256]{1,0:T(8,128)(2,1)} %wv_hbm.1, bf16[512,256]{1,0:T(8,128)(2,1)} %wg_hbm.1, ...), custom_call_target="tpu_custom_call" | custom-call | tf_op jit(solution)/shard_map/pallas_call | solution.py:1179
  42.1 0.7 %copy.21 = bf16[32,4,512]{2,1,0:T(4,128)(2,1)} copy(bf16[32,4,512]{2,1,0:T(4,128)(2,1)S(1)} %get-tuple-element.6) | data formatting | bytes 262144
  42.8 1.3 %copy.22 = f32[32,64,256]{2,1,0:T(8,128)} copy(f32[32,64,256]{2,1,0:T(8,128)S(1)} %bitcast.10) | data formatting | bytes 4194304

commit v4 on v3

--- a/solution.py
+++ b/solution.py
@@ -481,8 +481,8 @@
     tok_hbm, gain_hbm, wq_hbm, wk_hbm, wv_hbm, wg_hbm, wb_hbm, wd_hbm, base_hbm, og_hbm, wo_hbm,
     state_hbm, pk_hbm, pv_hbm, pb_hbm, pd_hbm, acc_hbm,
     mixed_ref, st,
-    gain_ref, wbd_ref, base_ref, og_ref, pk_ref, pv_ref, pb_ref, pd_ref, acc_ref, tok, wp, wo, normed, kq, res, tk, up, al, rows_a, rows_b, proj, own_part, part_send, part_recv, small_own, small_send, small_recv, send_buf, recv_buf, gate_buf, own_share,
-    in_sem, own_sem, wz_send, wz_recv, wy_send, wy_recv, t_send, f_send, d_send, t_recv, zr_send, zl_send, z_recv, y_send, y_recv, p_send, p_recv, r_send, r_recv,
+    gain_ref, wbd_ref, base_ref, og_ref, pkv_ref, pbd_ref, acc_ref, tok, wp, wo, normed, kq, res, tk, up, al, rows_a, rows_b, proj, own_part, part_send, part_recv, small_own, small_send, small_recv, send_buf, recv_buf, gate_buf, own_share,
+    in_sem, own_sem, wz_send, wz_recv, wy_send, wy_recv, t_send, f_send, d_send, t_recv, zs_send, z_recv, y_send, y_recv, p_send, p_recv, s_recv, r_send, r_recv,
     small_sem,
 ):
     n_grp, n_kv, n_tp, seqs, props, heads, hd = cfg
@@ -519,25 +519,28 @@
     for m in range(n_src + 1):
         if m < n_src:
             dst = wp.at[m, pl.ds(side * own_rows, own_rows), :]
-            copy = pltpu.make_async_copy(sources[m], dst, own_sem.at[m])
+            copy = pltpu.make_async_copy(sources[m], dst, own_sem.at[min(m, 1)])
         else:
-            copy = pltpu.make_async_copy(wo_hbm, wo.at[k], own_sem.at[m])
+            copy = pltpu.make_async_copy(wo_hbm, wo.at[k], own_sem.at[2])
         copy.start()
         own_copies.append(copy)
-    early, late = [], []
     ours = pl.ds(pl.multiple_of(pair * half_feats, half_feats), half_feats)
-    pairs = [
-        (pk_hbm, pk_ref, early), (pv_hbm, pv_ref, early), (pb_hbm, pb_ref, early),
-        (pd_hbm, pd_ref, early), (acc_hbm, acc_ref, early),
-        (gain_hbm.at[:, ours], gain_ref, late),
-        (wb_hbm.at[:, ours], wbd_ref.at[pl.ds(0, all_heads), :], late),
-        (wd_hbm.at[:, ours], wbd_ref.at[pl.ds(all_heads, all_heads), :], late),
-        (base_hbm, base_ref, late), (og_hbm, og_ref, late),
+    loads = [
+        (pk_hbm, pkv_ref.at[0], 0), (pv_hbm, pkv_ref.at[1], 0),
+        (pb_hbm, pbd_ref.at[0], 1), (pd_hbm, pbd_ref.at[1], 1), (acc_hbm, acc_ref, 2),
+        (wb_hbm.at[:, ours], wbd_ref.at[pl.ds(0, all_heads), :], 3),
+        (wd_hbm.at[:, ours], wbd_ref.at[pl.ds(all_heads, all_heads), :], 3),
+        (gain_hbm.at[:, ours], gain_ref, 4), (base_hbm, base_ref, 5), (og_hbm, og_ref, 6),
     ]
-    for i, (src, dst, group) in enumerate(pairs):
-        copy = pltpu.make_async_copy(src, dst, small_sem.at[i])
-        copy.start()
-        group.append(copy)
+    for src, dst, i in loads:
+        pltpu.make_async_copy(src, dst, small_sem.at[i]).start()
+    early = [(pkv_ref, 0), (pbd_ref, 1), (acc_ref, 2)]
+    late = [(wbd_ref, 3), (gain_ref, 4), (base_ref, 5), (og_ref, 6)]
+
+    def loaded(group):
+        for ref, i in group:
+            pltpu.make_async_copy(ref, ref, small_sem.at[i]).wait()
+
     state_in = pltpu.make_async_copy(state_hbm, st, in_sem.at[1])
     state_in.start()
 
@@ -565,39 +568,43 @@
 
     def tok_partner():
         return remote(tok_piece(4, 0), tok_piece(core, 0), t_send.at[0],
-                      t_recv.at[core, 0], {"kv": partner})
+                      t_recv.at[2 * core], {"kv": partner})
 
     def tok_shift():
-        return remote(tok_piece(4, 1), tok_piece(5, 1), t_send.at[1], t_recv.at[4, 1],
+        return remote(tok_piece(4, 1), tok_piece(5, 1), t_send.at[1], t_recv.at[6],
                       {"tp": far_tp})
 
     def tok_relay():
         return remote(tok_piece(5, 1), tok_piece(core, 1), t_send.at[0],
-                      t_recv.at[core, 1], {"kv": partner})
-
-    def tok_far(slot, half):
-        ref = tok_piece(slot, half)
-        return remote(ref, ref, f_send.at[slot // 2, half], t_recv.at[slot, half],
-                      {"tp": far_tp})
-
-    def tok_beside(slot, half):
-        ref = tok_piece(slot, half)
-        return remote(ref, ref, d_send.at[slot // 2, half], t_recv.at[slot, half],
-                      {"tp": beside_core})
-
-    def tok_wait(slot, half):
-        ref = tok_piece(slot, half)
-        remote(ref, ref, d_send.at[0, half], t_recv.at[slot, half],
-               {"tp": beside_core}).wait_recv()
+                      t_recv.at[2 * core + 1], {"kv": partner})
+
+    def tok_far(half):
+        ref = tok_piece(core, half)
+        return remote(ref, ref, f_send.at[0], t_recv.at[2 * core + half], {"tp": far_tp})
+
+    def tok_beside(half):
+        ref = tok_piece(core, half)
+        return remote(ref, ref, d_send.at[0], t_recv.at[2 * core + half], {"tp": beside_core})
+
+    def own_far():
+        ref = tok.at[2 + core]
+        return remote(ref, ref, f_send.at[1], t_recv.at[4 + core], {"tp": far_tp})
+
+    def own_beside():
+        ref = tok.at[2 + core]
+        return remote(ref, ref, d_send.at[0], t_recv.at[4 + core], {"tp": beside_core})
+
+    def tok_wait(ref, index):
+        remote(ref, ref, d_send.at[0], t_recv.at[index], {"tp": beside_core}).wait_recv()
 
     def tok_land_z():
-        tok_wait(core, 1 - home)
-        tok_far(core, 1 - home).start()
-        tok_beside(core, 1 - home).start()
+        tok_wait(tok_piece(core, 1 - home), 2 * core + 1 - home)
+        tok_far(1 - home).start()
+        tok_beside(1 - home).start()
 
     def tok_land_x():
-        tok_wait(core, home)
-        tok_beside(core, home).start()
+        tok_wait(tok_piece(core, home), 2 * core + home)
+        tok_beside(home).start()
 
     def w_slot(m, block, half, bit):
         at = pl.ds(block * own_rows + half * piece + bit * (piece // w_bits), piece // w_bits)
@@ -605,43 +612,41 @@
 
     def w_mate(m, bit):
         ref = w_slot(m, side, g, bit)
-        return remote(ref, ref, wz_send.at[m, bit], wz_recv.at[m, bit], {"kv": mate})
+        return remote(ref, ref, wz_send.at[0], wz_recv.at[m, bit], {"kv": mate})
 
     def w_share(m, bit):
         ref = w_slot(m, 1 - side, g, bit)
-        return remote(ref, ref, wy_send.at[m, bit], wy_recv.at[m, bit], {"grp": g_other})
+        return remote(ref, ref, wy_send.at[0], wy_recv.at[m], {"grp": g_other})
 
     def w_pass(m):
         for bit in range(w_bits):
             ref = w_slot(m, 1 - side, g, bit)
-            remote(ref, ref, wz_send.at[m, bit], wz_recv.at[m, bit], {"kv": mate}).wait_recv()
+            remote(ref, ref, wz_send.at[0], wz_recv.at[m, bit], {"kv": mate}).wait_recv()
             w_share(m, bit).start()
 
     def w_ready(m):
-        for bit in range(w_bits):
-            ref = w_slot(m, 1 - side, g_other, bit)
-            remote(ref, ref, wy_send.at[m, bit], wy_recv.at[m, bit], {"grp": g_other}).wait_recv()
+        at = pl.ds((1 - side) * own_rows + g_other * piece, piece)
+        ref = wp.at[m, at, :]
+        remote(ref, ref, wy_send.at[0], wy_recv.at[m], {"grp": g_other}).wait_recv()
 
     def o_slot(origin, part, bit):
         return wo.at[origin, pl.ds(part * out_piece + bit * out_bit, out_bit), :]
 
     def z_right(origin, bit):
         ref = o_slot(origin, g, bit)
-        return remote(ref, ref, zr_send.at[origin, bit], z_recv.at[origin, bit], {"kv": k + 1})
+        return remote(ref, ref, zs_send.at[1 - pair], z_recv.at[origin, bit], {"kv": k + 1})
 
     def z_left(origin, bit):
         ref = o_slot(origin, g, bit)
-        return remote(ref, ref, zl_send.at[origin, bit], z_recv.at[origin, bit], {"kv": k - 1})
+        return remote(ref, ref, zs_send.at[pair], z_recv.at[origin, bit], {"kv": k - 1})
 
     def y_copy(origin, bit):
         ref = o_slot(origin, g, bit)
-        return remote(ref, ref, y_send.at[origin, bit], y_recv.at[origin, bit], {"grp": g_other})
+        return remote(ref, ref, y_send.at[0], y_recv.at[origin], {"grp": g_other})
 
     def y_wait(origin):
-        for bit in range(out_bits):
-            ref = o_slot(origin, g_other, bit)
-            remote(ref, ref, y_send.at[origin, bit], y_recv.at[origin, bit],
-                   {"grp": g_other}).wait_recv()
+        ref = wo.at[origin, pl.ds(g_other * out_piece, out_piece), :]
+        remote(ref, ref, y_send.at[0], y_recv.at[origin], {"grp": g_other}).wait_recv()
 
     def right_start(origin):
         for bit in range(out_bits):
@@ -695,24 +700,25 @@
         def _():
             share_out(k + 1 if s == 0 else k - s)
 
-    def end_pass(s):
-        @pl.when(k == 0)
-        def _():
-            from_right(k + s)
-            share_out(k + s)
-
-        @pl.when(k == n_kv - 1)
-        def _():
-            from_left(k - s)
-            share_out(k - s)
+    def end_pass(s, bits=(0, 1)):
+        for bit in bits:
+            @pl.when(k == 0)
+            def _():
+                z_left(k + s, bit).wait_recv()
+                y_copy(k + s, bit).start()
+
+            @pl.when(k == n_kv - 1)
+            def _():
+                z_right(k - s, bit).wait_recv()
+                y_copy(k - s, bit).start()
 
     def p_copy(m, b):
         at = pl.ds(b * half_rows, half_rows)
-        return remote(part_send.at[m, at], part_recv.at[m, at], p_send.at[m, b],
+        return remote(part_send.at[m, at], part_recv.at[m, at], p_send.at[0],
                       p_recv.at[m, b], {"kv": partner})
 
     def small_copy():
-        return remote(small_send, small_recv, p_send.at[n_src, 0], p_recv.at[n_src, 0],
+        return remote(small_send, small_recv, p_send.at[1], s_recv.at[0],
                       {"kv": partner})
 
     at_end = jnp.logical_or(k == 0, k == n_kv - 1)
@@ -725,15 +731,14 @@
 
     @pl.when(home == 1)
     def _():
-        for half in range(2):
-            tok_far(2 + core, half).start()
-            tok_beside(2 + core, half).start()
+        own_far().start()
+        own_beside().start()
 
     def w_first(m):
-        own_copies[m].wait()
         for bit in range(w_bits):
             w_mate(m, bit).start()
 
+    own_copies[0].wait()
     w_first(0)
     own_copies[n_src].wait()
 
@@ -746,9 +751,10 @@
         def _():
             left_start(k)
 
-        w_first(1)
-        w_first(2)
-        w_first(3)
+        rest = wp.at[pl.ds(1, n_src - 1), pl.ds(side * own_rows, own_rows), :]
+        pltpu.make_async_copy(rest, rest, own_sem.at[1]).wait()
+        for m in range(1, n_src):
+            w_first(m)
 
     relays_first = jnp.logical_and(at_end, home == 1)
 
@@ -846,11 +852,10 @@
     def split(ref):
         return [rd(ref, pl.ds(t, seqs, stride=props)) for t in range(props)]
 
-    for copy in early:
-        copy.wait()
-    pk = pk_ref[...].astype(F32).reshape(rows, width)
+    loaded(early)
+    pk = pkv_ref[0].astype(F32).reshape(rows, width)
     wr(rows_a, every, pk * lax.rsqrt(head_sum(pk * pk) + EPS))
-    wr(rows_b, every, pv_ref[...].astype(F32).reshape(rows, width))
+    wr(rows_b, every, pkv_ref[1].astype(F32).reshape(rows, width))
     keys = split(rows_a)
     values = split(rows_b)
     own_head = (
@@ -866,8 +871,8 @@
     weights, logs = [], []
     for t in range(props):
         live = (acc_ref[...] > t).astype(F32)
-        weights.append(over_lanes(jax.nn.sigmoid(pb_ref[t]) * live))
-        logs.append(over_lanes(pd_ref[t] * live))
+        weights.append(over_lanes(jax.nn.sigmoid(pbd_ref[0, t]) * live))
+        logs.append(over_lanes(pbd_ref[1, t] * live))
         put_heads(kq, keys[t], t, pad)
         put_heads(kq, keys[t], props + t, pad)
     state_in.wait()
@@ -891,8 +896,7 @@
 
     @pl.when(home == 1)
     def _():
-        remote(tok_piece(5, 1), tok_piece(5, 1), t_send.at[1], t_recv.at[4, 1],
-               {"tp": far_tp}).wait_recv()
+        tok_wait(tok_piece(5, 1), 6)
         tok_relay().start()
 
     @pl.when(relays_first)
@@ -901,9 +905,8 @@
 
     @pl.when(home == 0)
     def _():
-        for half in range(2):
-            tok_wait(2 + core, half)
-            tok_beside(2 + core, half).start()
+        tok_wait(tok.at[2 + core], 4 + core)
+        own_beside().start()
 
     @pl.when(home == 1)
     def _():
@@ -931,11 +934,10 @@
     w_pass(1)
     middle_pass(1)
 
-    for copy in late:
-        copy.wait()
+    loaded(late)
+    tok_wait(tok.at[3 - core], 5 - core)
     for half in range(2):
-        tok_wait(3 - core, half)
-        tok_wait(1 - core, half)
+        tok_wait(tok_piece(1 - core, half), 2 * (1 - core) + half)
     ones = jnp.ones((8, feats), BF16)
     squares = jnp.zeros((8, 2 * rows), F32)
     last = (((1,), (1,)), ((), ()))
@@ -986,15 +988,15 @@
     end_pass(1)
     middle_share(1)
     middle_share(2)
+    lax.fori_loop(0, seqs // 2, renew, 0, unroll=4)
     w_ready(2)
     project(2)
     give((2, 0), (1, 1))
-    lax.fori_loop(0, seqs // 2, renew, 0, unroll=4)
+    lax.fori_loop(seqs // 2, seqs, renew, 0, unroll=4)
     w_ready(3)
     project(3)
     give((3, 0), (2, 1), (3, 1))
     end_pass(2)
-    lax.fori_loop(seqs // 2, seqs, renew, 0, unroll=4)
 
     small_copy().wait_recv()
     small = small_own[...] + small_recv[...]
@@ -1027,13 +1029,14 @@
 
     def r_copy(dest, b):
         at = pl.ds(b * half_rows, half_rows)
-        return remote(send_buf.at[dest, at], recv_buf.at[t_me, at], r_send.at[dest, b],
-                      r_recv.at[t_me, b], {"tp": dest})
-
-    def r_wait(origin, b):
-        at = pl.ds(b * half_rows, half_rows)
-        remote(send_buf.at[origin, at], recv_buf.at[origin, at], r_send.at[origin, b],
-               r_recv.at[origin, b], {"tp": origin}).wait_recv()
+        far = lax.rem(dest - t_me + n_tp, n_tp)
+        return remote(send_buf.at[dest, at], recv_buf.at[t_me, at], r_send.at[0],
+                      r_recv.at[far - 1, b], {"tp": dest})
+
+    def r_wait(d, b):
+        origin = lax.rem(t_me + n_tp - d, n_tp)
+        ref = recv_buf.at[origin, pl.ds(b * half_rows, half_rows)]
+        remote(ref, ref, r_send.at[0], r_recv.at[d - 1, b], {"tp": origin}).wait_recv()
 
     def send_share(dest, b):
         at = slice(b * half_rows, (b + 1) * half_rows)
@@ -1061,6 +1064,8 @@
         steps = [pl.ds(first + t, count, stride=props) for t in range(props)]
         for m in range(3):
             finish(m, b)
+            if b == 0 and m == 1:
+                end_pass(3, (0,))
         keys, queries, values = [[rd(proj, at, m) for at in steps] for m in range(3)]
         weights = [rd(rows_a, at) for at in steps]
         logs = [rd(rows_b, at) for at in steps]
@@ -1068,6 +1073,8 @@
             put_heads(kq, keys[t], t, pad, low)
             put_heads(kq, queries[t], props + t, pad, low)
         lax.fori_loop(low, low + count, by_state, 0, unroll=4)
+        if b == 0:
+            end_pass(3, (1,))
         outs = solve(keys, values, weights, logs, queries, low)[3]
         for t in range(props):
             wr(rows_a, steps[t], outs[t])
@@ -1104,67 +1111,51 @@
         at = slice(b * half_rows, (b + 1) * half_rows)
         total = own_share[at]
         for d in range(1, n_tp):
-            origin = lax.rem(t_me + d, n_tp)
-            r_wait(origin, b)
-            total = total + recv_buf[origin, at].astype(F32)
+            r_wait(d, b)
+            total = total + recv_buf[lax.rem(t_me + n_tp - d, n_tp), at].astype(F32)
         mixed_ref[b * count : (b + 1) * count] = total.reshape(count, props, feats).astype(BF16)
 
     delta(0)
-    end_pass(3)
-    lax.fori_loop(0, n_kv // 2, take(0), 0)
+    lax.fori_loop(0, n_kv - 1, take(0), 0)
     delta(1)
-    lax.fori_loop(n_kv // 2, n_kv - 1, take(0), 0)
     lax.fori_loop(0, n_kv - 1, take(1), 0)
     lax.fori_loop(n_kv - 1, n_kv, take(0), 0)
     lax.fori_loop(n_kv - 1, n_kv, take(1), 0)
+    def sent(ref, sem):
+        remote(ref, ref, sem, s_recv.at[0], {"kv": mate}).wait_send()
+
+    sent(tok.at[pl.ds(0, 2)], d_send.at[0])
+    tok_far(1 - home).wait_send()
+
+    @pl.when(home == 1)
+    def _():
+        own_far().wait_send()
+        tok_relay().wait_send()
+
+    @pl.when(home == 0)
+    def _():
+        tok_partner().wait_send()
+        tok_shift().wait_send()
+
+    sent(wp.at[0], wz_send.at[0])
+    sent(wp.at[0], wy_send.at[0])
+    sent(part_send, p_send.at[0])
+    sent(small_send, p_send.at[1])
+    some = pl.ds(0, out_piece)
+    sent(wo.at[pl.ds(0, n_kv - 1), some], y_send.at[0])
+
+    @pl.when(at_end)
+    def _():
+        sent(wo.at[0, some], zs_send.at[1])
+
+    @pl.when(jnp.logical_not(at_end))
+    def _():
+        sent(wo.at[pl.ds(0, 3), some], zs_send.at[0])
+        sent(wo.at[pl.ds(0, 2), some], zs_send.at[1])
+
     settle(0)
     settle(1)
-
-    for half in range(2):
-        tok_beside(core, half).wait_send()
-        tok_beside(2 + core, half).wait_send()
-    tok_far(core, 1 - home).wait_send()
-
-    @pl.when(home == 1)
-    def _():
-        tok_far(2 + core, 0).wait_send()
-        tok_far(2 + core, 1).wait_send()
-        tok_relay().wait_send()
-
-    @pl.when(home == 0)
-    def _():
-        tok_partner().wait_send()
-        tok_shift().wait_send()
-
-    for m in range(n_src):
-        for bit in range(w_bits):
-            w_mate(m, bit).wait_send()
-            w_share(m, bit).wait_send()
-        p_copy(m, 0).wait_send()
-        p_copy(m, 1).wait_send()
-    small_copy().wait_send()
-    for d in range(1, n_tp):
-        r_copy(lax.rem(t_me + d, n_tp), 0).wait_send()
-        r_copy(lax.rem(t_me + d, n_tp), 1).wait_send()
-
-    def drain(o, carry):
-        for bit in range(out_bits):
-            @pl.when(jnp.logical_and(o <= k, k < n_kv - 1))
-            def _():
-                z_right(o, bit).wait_send()
-
-            @pl.when(jnp.logical_and(o >= k, k > 0))
-            def _():
-                z_left(o, bit).wait_send()
-
-            @pl.when(o != k)
-            def _():
-                y_copy(o, bit).wait_send()
-
-        return carry
-
-    lax.fori_loop(0, n_kv, drain, 0)
-
+    sent(send_buf.at[pl.ds(0, n_tp - 1)], r_send.at[0])
 
 def pair_call(sizes, args, seqs, props, feats, heads, hd, width, rows, pad):
     n_grp, n_kv, n_tp = sizes
@@ -1187,7 +1178,9 @@
         scratch_shapes=[
             pltpu.VMEM((1, 2 * feats), F32),
             pltpu.VMEM((2 * all_heads, 2 * feats), BF16),
-            *[pltpu.VMEM(args[i].shape, args[i].dtype) for i in (8, 9, 12, 13, 14, 15, 16)],
+            *[pltpu.VMEM(args[i].shape, args[i].dtype) for i in (8, 9)],
+            *[pltpu.VMEM((2, *args[i].shape), args[i].dtype) for i in (12, 14)],
+            pltpu.VMEM(args[16].shape, args[16].dtype),
             pltpu.VMEM((6, seqs, props, feats), BF16),
             pltpu.VMEM((n_src, 2 * own_rows, width), BF16),
             pltpu.VMEM((n_tp, width, feats), BF16),
@@ -1211,18 +1204,25 @@
             pltpu.VMEM((rows, width), BF16),
             pltpu.VMEM((rows, feats), F32),
             dma((2,)),
-            dma((n_src + 1,)),
-            *[dma((n_src, 2)) for _ in range(4)],
+            dma((3,)),
+            dma((1,)),
+            dma((n_src, 2)),
+            dma((1,)),
+            dma((n_src,)),
             dma((2,)),
-            dma((2, 2)),
-            dma((2, 2)),
-            dma((5, 2)),
-            *[dma((n_kv, 2)) for _ in range(5)],
-            dma((n_src + 1, 2)),
-            dma((n_src + 1, 2)),
-            dma((n_tp, 2)),
-            dma((n_tp, 2)),
-            dma((10,)),
+            dma((2,)),
+            dma((1,)),
+            dma((7,)),
+            dma((2,)),
+            dma((n_kv, 2)),
+            dma((1,)),
+            dma((n_kv,)),
+            dma((2,)),
+            dma((n_src, 2)),
+            dma((1,)),
+            dma((1,)),
+            dma((n_tp - 1, 2)),
+            dma((7,)),
         ],
         compiler_params=pltpu.CompilerParams(
             collective_id=1, has_side_effects=True, vmem_limit_bytes=67043328 - rows * feats * 2 - seqs * hd * width * 4),

time: 44.2 us -> 42.8 us (0.968)
  Pallas kernels: 41.5 us -> 40.1 us
    pallas_call x1, Pallas kernels: 41.5 us -> 40.1 us  [pair_call(): pl.pallas_call(functools.partial(pair_kernel, cfg), out_shape=(pltpu.VMEM...]
where the time goes in v4:
time: 42.8 us; the launch traced here: 42.7 us
  Pallas kernels  40.1 us (94%)
  local copies, waits for them, and re-layouts  1.98 us (5%)
  between operations  0.65 us (2%)
    pallas_call x1, Pallas kernels, pair_call(): pl.pallas_call(functools.partial(pair_kernel, cfg), out_shape=(pltpu.VMEM...  40.1 us
    unnamed x2, local copies, waits for them, and re-layouts  1.98 us

profile of v4, /device:TPU:0, one launch (start us, length us, event | category | flops | bytes accessed | tf_op | source)
XLA Modules:
  0.0 42.7 jit_solution(17855378403384079699)
XLA Ops:
  0.6 40.1 %shard_map.176 = (bf16[32,4,512]{2,1,0:T(4,128)(2,1)S(1)}, f32[2048,256]{1,0:T(8,128)S(1)}) custom-call(bf16[32,4,512]{2,1,0:T(4,128)(2,1)} %tok_hbm.1, f32[1,2048]{1,0:T(1,128)} %bitcast.14, bf16[512,256]{1,0:T(8,128)(2,1)} %wq_hbm.1, bf16[512,256]{1,0:T(8,128)(2,1)} %wk_hbm.1, bf16[512,256]{1,0:T(8,128)(2,1)} %wv_hbm.1, bf16[512,256]{1,0:T(8,128)(2,1)} %wg_hbm.1, ...), custom_call_target="tpu_custom_call" | custom-call | tf_op jit(solution)/shard_map/pallas_call | solution.py:1170
  40.7 0.7 %copy.21 = bf16[32,4,512]{2,1,0:T(4,128)(2,1)} copy(bf16[32,4,512]{2,1,0:T(4,128)(2,1)S(1)} %get-tuple-element.6) | data formatting | bytes 262144
  41.4 1.3 %copy.22 = f32[32,64,256]{2,1,0:T(8,128)} copy(f32[32,64,256]{2,1,0:T(8,128)S(1)} %bitcast.10) | data formatting | bytes 4194304

commit v5 on v4

--- a/solution.py
+++ b/solution.py
@@ -482,7 +482,7 @@
     state_hbm, pk_hbm, pv_hbm, pb_hbm, pd_hbm, acc_hbm,
     mixed_ref, st,
     gain_ref, wbd_ref, base_ref, og_ref, pkv_ref, pbd_ref, acc_ref, tok, wp, wo, normed, kq, res, tk, up, al, rows_a, rows_b, proj, own_part, part_send, part_recv, small_own, small_send, small_recv, send_buf, recv_buf, gate_buf, own_share,
-    in_sem, own_sem, wz_send, wz_recv, wy_send, wy_recv, t_send, f_send, d_send, t_recv, zs_send, z_recv, y_send, y_recv, p_send, p_recv, s_recv, r_send, r_recv,
+    in_sem, own_sem, wz_send, wz_recv, wy_recv, t_send, f_send, d_send, t_recv, zs_send, z_recv, y_send, y_recv, p_send, p_recv, s_recv, r_recv,
     small_sem,
 ):
     n_grp, n_kv, n_tp, seqs, props, heads, hd = cfg
@@ -616,7 +616,7 @@
 
     def w_share(m, bit):
         ref = w_slot(m, 1 - side, g, bit)
-        return remote(ref, ref, wy_send.at[0], wy_recv.at[m], {"grp": g_other})
+        return remote(ref, ref, wz_send.at[0], wy_recv.at[m], {"grp": g_other})
 
     def w_pass(m):
         for bit in range(w_bits):
@@ -627,7 +627,7 @@
     def w_ready(m):
         at = pl.ds((1 - side) * own_rows + g_other * piece, piece)
         ref = wp.at[m, at, :]
-        remote(ref, ref, wy_send.at[0], wy_recv.at[m], {"grp": g_other}).wait_recv()
+        remote(ref, ref, wz_send.at[0], wy_recv.at[m], {"grp": g_other}).wait_recv()
 
     def o_slot(origin, part, bit):
         return wo.at[origin, pl.ds(part * out_piece + bit * out_bit, out_bit), :]
@@ -715,7 +715,7 @@
     def p_copy(m, b):
         at = pl.ds(b * half_rows, half_rows)
         return remote(part_send.at[m, at], part_recv.at[m, at], p_send.at[0],
-                      p_recv.at[m, b], {"kv": partner})
+                      p_recv.at[max(m, 1) - 1, b], {"kv": partner})
 
     def small_copy():
         return remote(small_send, small_recv, p_send.at[1], s_recv.at[0],
@@ -983,8 +983,8 @@
     w_ready(1)
     project(1)
     give((1, 0))
+    w_pass(3)
     middle_pass(2)
-    w_pass(3)
     end_pass(1)
     middle_share(1)
     middle_share(2)
@@ -1018,7 +1018,11 @@
         scale, (lax.broadcasted_iota(jnp.int32, (scale.shape[0], width), 0) == 0).astype(F32))
 
     def finish(m, b):
-        p_copy(m, b).wait_recv()
+        if m == 0:
+            ref = part_recv.at[pl.ds(0, 2), pl.ds(b * half_rows, half_rows)]
+            remote(ref, ref, p_send.at[0], p_recv.at[0, b], {"kv": partner}).wait_recv()
+        elif m > 1:
+            p_copy(m, b).wait_recv()
         at = slice(b * half_rows, (b + 1) * half_rows)
         value = (own_part[m, at] + part_recv[m, at].astype(F32)) * row_scale[at]
         if m == 0:
@@ -1029,14 +1033,13 @@
 
     def r_copy(dest, b):
         at = pl.ds(b * half_rows, half_rows)
-        far = lax.rem(dest - t_me + n_tp, n_tp)
-        return remote(send_buf.at[dest, at], recv_buf.at[t_me, at], r_send.at[0],
-                      r_recv.at[far - 1, b], {"tp": dest})
-
-    def r_wait(d, b):
-        origin = lax.rem(t_me + n_tp - d, n_tp)
-        ref = recv_buf.at[origin, pl.ds(b * half_rows, half_rows)]
-        remote(ref, ref, r_send.at[0], r_recv.at[d - 1, b], {"tp": origin}).wait_recv()
+        far = lax.rem(t_me - dest + n_tp, n_tp)
+        return remote(send_buf.at[dest, at], recv_buf.at[far - 1, at], y_send.at[0],
+                      r_recv.at[b], {"tp": dest})
+
+    def r_wait(b):
+        ref = recv_buf.at[pl.ds(0, n_tp - 1), pl.ds(b * half_rows, half_rows)]
+        remote(ref, ref, y_send.at[0], r_recv.at[b], {"tp": beside_core}).wait_recv()
 
     def send_share(dest, b):
         at = slice(b * half_rows, (b + 1) * half_rows)
@@ -1109,10 +1112,10 @@
 
     def settle(b):
         at = slice(b * half_rows, (b + 1) * half_rows)
+        r_wait(b)
         total = own_share[at]
         for d in range(1, n_tp):
-            r_wait(d, b)
-            total = total + recv_buf[lax.rem(t_me + n_tp - d, n_tp), at].astype(F32)
+            total = total + recv_buf[d - 1, at].astype(F32)
         mixed_ref[b * count : (b + 1) * count] = total.reshape(count, props, feats).astype(BF16)
 
     delta(0)
@@ -1137,12 +1140,10 @@
         tok_partner().wait_send()
         tok_shift().wait_send()
 
-    sent(wp.at[0], wz_send.at[0])
-    sent(wp.at[0], wy_send.at[0])
+    sent(wp.at[pl.ds(0, 2)], wz_send.at[0])
     sent(part_send, p_send.at[0])
     sent(small_send, p_send.at[1])
     some = pl.ds(0, out_piece)
-    sent(wo.at[pl.ds(0, n_kv - 1), some], y_send.at[0])
 
     @pl.when(at_end)
     def _():
@@ -1155,7 +1156,7 @@
 
     settle(0)
     settle(1)
-    sent(send_buf.at[pl.ds(0, n_tp - 1)], r_send.at[0])
+    sent(wo.at[pl.ds(0, n_kv - 1)], y_send.at[0])
 
 def pair_call(sizes, args, seqs, props, feats, heads, hd, width, rows, pad):
     n_grp, n_kv, n_tp = sizes
@@ -1207,7 +1208,6 @@
             dma((3,)),
             dma((1,)),
             dma((n_src, 2)),
-            dma((1,)),
             dma((n_src,)),
             dma((2,)),
             dma((2,)),
@@ -1218,10 +1218,9 @@
             dma((1,)),
             dma((n_kv,)),
             dma((2,)),
-            dma((n_src, 2)),
+            dma((n_src - 1, 2)),
             dma((1,)),
-            dma((1,)),
-            dma((n_tp - 1, 2)),
+            dma((2,)),
             dma((7,)),
         ],
         compiler_params=pltpu.CompilerParams(

time: 42.8 us -> 42.8 us (level)
  no operation moved by 1% of the time
where the time goes in v5:
time: 42.8 us; the launch traced here: 42.7 us
  Pallas kernels  40 us (93%)
  local copies, waits for them, and re-layouts  1.98 us (5%)
  between operations  0.65 us (2%)
    pallas_call x1, Pallas kernels, pair_call(): pl.pallas_call(functools.partial(pair_kernel, cfg), out_shape=(pltpu.VMEM...  40 us
    unnamed x2, local copies, waits for them, and re-layouts  1.98 us

profile of v5, /device:TPU:0, one launch (start us, length us, event | category | flops | bytes accessed | tf_op | source)
XLA Modules:
  0.0 42.7 jit_solution(10862598062586044516)
XLA Ops:
  0.6 40.0 %shard_map.176 = (bf16[32,4,512]{2,1,0:T(4,128)(2,1)S(1)}, f32[2048,256]{1,0:T(8,128)S(1)}) custom-call(bf16[32,4,512]{2,1,0:T(4,128)(2,1)} %tok_hbm.1, f32[1,2048]{1,0:T(1,128)} %bitcast.14, bf16[512,256]{1,0:T(8,128)(2,1)} %wq_hbm.1, bf16[512,256]{1,0:T(8,128)(2,1)} %wk_hbm.1, bf16[512,256]{1,0:T(8,128)(2,1)} %wv_hbm.1, bf16[512,256]{1,0:T(8,128)(2,1)} %wg_hbm.1, ...), custom_call_target="tpu_custom_call" | custom-call | tf_op jit(solution)/shard_map/pallas_call | solution.py:1171
  40.7 0.7 %copy.21 = bf16[32,4,512]{2,1,0:T(4,128)(2,1)} copy(bf16[32,4,512]{2,1,0:T(4,128)(2,1)S(1)} %get-tuple-element.6) | data formatting | bytes 262144
  41.3 1.3 %copy.22 = f32[32,64,256]{2,1,0:T(8,128)} copy(f32[32,64,256]{2,1,0:T(8,128)S(1)} %bitcast.10) | data formatting | bytes 4194304
